TPU v7x, 32 devices: a whole 2x2x4 slice. The times are simulated.
32 devices in a mesh: row: 8 (over z, x), col: 4 (over y, core).
Axes of the slice: x: 2, y: 2, z: 4, core: 2. Of those that a mesh axis runs over, the one named last changes fastest.
Arguments:
- tokens: bfloat16 [2, 32768, 2048], P(None, ('row', 'col')), may hold values from -6 to 6
- norm_gain: float32 [2048], replicated, may hold values from 0.1 to 1.9
- mix_weight: bfloat16 [2048, 1024], replicated, may hold values from -0.125 to 0.125
- gate_weight: bfloat16 [2048, 2048], replicated, may hold values from -0.125 to 0.125
- out_weight: bfloat16 [1024, 2048], replicated, may hold values from -0.1875 to 0.1875
Outputs:
- gated: bfloat16 [2, 32768, 2048], P(None, ('row', 'col'))
All inputs are finite; a program needn't handle non-finite values.
Results may differ from a plain program's by a relative error of at most 0.017.
Values may be sent and summed in bfloat16 or wider, within the bound.
A program may use at most 128 MiB of HBM per device.

v0:
```python
import functools
import math

import jax
import jax.numpy as jnp
import numpy as np
from jax import lax
from jax.experimental import pallas as pl
from jax.experimental.pallas import tpu as pltpu
from jax.sharding import PartitionSpec as P

GROUP_DIM = 128
HALF = GROUP_DIM // 2
BF16 = jnp.bfloat16
F32 = jnp.float32
AXES = ("row", "col")
LANES = 128
STEP = 8


def angles(left, right, period):
    return (np.outer(left, right) % period) * (2.0 * math.pi / period)


def channel_table():
    phase = angles(np.arange(GROUP_DIM), np.arange(HALF), GROUP_DIM)
    table = np.stack([np.cos(phase), np.sin(phase)], axis=-1)
    table[:, 0, 1] = np.cos(math.pi * np.arange(GROUP_DIM))
    return table.reshape(GROUP_DIM, GROUP_DIM) * GROUP_DIM ** -0.5


def channel_order():
    order = np.zeros((HALF, 2), np.int64)
    order[:, 0] = np.arange(HALF)
    order[:, 1] = GROUP_DIM - np.arange(HALF)
    order[0, 1] = HALF
    pick = np.zeros((GROUP_DIM, GROUP_DIM))
    pick[np.arange(GROUP_DIM), order.reshape(-1)] = 1.0
    return pick


def position_tables(devices, length, first):
    second, fold = length // first, first // devices
    phase = angles(np.arange(first), np.arange(first), first)
    cosine, sine = np.cos(phase), np.sin(phase)
    zero = np.zeros_like(cosine)
    from_left = np.concatenate([cosine, sine, cosine, sine], axis=1)
    from_right = np.concatenate([-sine, cosine, sine, -cosine], axis=1)
    lone_left = np.concatenate([cosine, sine, zero, zero], axis=1)
    lone_right = np.concatenate([zero, zero, cosine, sine], axis=1)

    def interleave(left, right):
        pair = np.stack([left, right]).reshape(2, devices, fold, -1).transpose(0, 2, 1, 3)
        return pair.reshape(2 * first, 4 * first)

    turn = angles(np.arange(second), np.arange(first), length)
    last = angles(np.arange(second), np.arange(second), second)
    closing = np.concatenate([np.cos(last), -np.sin(last)], axis=1) * length ** -0.5
    return (
        interleave(from_left, from_right),
        interleave(lone_left, lone_right),
        np.cos(turn),
        np.sin(turn),
        closing,
    )


def turn_halves(u, cosine, sine, first):
    halves = []
    for half in range(2):
        real = u[..., 2 * half * first : (2 * half + 1) * first]
        imag = u[..., (2 * half + 1) * first : (2 * half + 2) * first]
        halves.append(
            jnp.concatenate(
                [(real * cosine - imag * sine).astype(BF16), (real * sine + imag * cosine).astype(BF16)], axis=-2
            )
        )
    return jnp.concatenate(halves, axis=-1)


def transform_kernel(first, x_ref, g_ref, cos_ref, sin_ref, close_ref, out_ref, rows_in, rows_out):
    devices, channels, here = x_ref.shape
    second = cos_ref.shape[0]
    fold, tiles = here // second, second // LANES
    for tile in range(here // LANES):
        rows_in[tile] = (
            x_ref[:, :, tile * LANES : (tile + 1) * LANES].astype(F32).reshape(devices * channels, LANES)
        )
    cosine, sine = cos_ref[...], sin_ref[...]
    for pair in range(channels // 2):
        rows = []
        for column in range(2):
            for high in range(fold):
                picked = pl.ds(2 * pair + column, devices, stride=channels)
                rows.append(
                    jnp.concatenate(
                        [rows_in[high * tiles + tile, picked, :] for tile in range(tiles)], axis=1
                    ).astype(BF16)
                )
        x = jnp.concatenate(rows, axis=0)
        g = g_ref[0] if pair == 0 else g_ref[1]
        if pair == 0:
            g = jnp.where(pl.program_id(0) == 0, g, g_ref[1])
        u = lax.dot_general(x, g, (((0,), (0,)), ((), ())), preferred_element_type=F32)
        turned = turn_halves(u, cosine, sine, first)
        y = jnp.dot(close_ref[...], turned, preferred_element_type=F32)
        for half in range(2):
            rows_out[pl.ds(2 * pair + half, second, stride=channels), :] = y[:, half * first : (half + 1) * first]
    out_ref[...] = rows_out[...].reshape(out_ref.shape).astype(BF16)


def position_transform(x, lone_here, devices, length, first):
    _, channels, here = x.shape
    second, fold = length // first, first // devices
    normal, lone, cosine, sine, closing = position_tables(devices, length, first)
    normal, lone = jnp.asarray(normal, BF16), jnp.asarray(lone, BF16)
    cosine, sine, closing = jnp.asarray(cosine, F32), jnp.asarray(sine, F32), jnp.asarray(closing, BF16)
    g = jnp.stack([jnp.where(lone_here, lone, normal), normal])
    if not fits(channels, here, first, devices):
        pairs, span = channels // 2, min(first, here)
        x = x.reshape(devices, pairs, 2, fold, second).transpose(1, 2, 3, 0, 4).reshape(pairs, 2 * first, second)
        g = jnp.stack([g[min(pair, 1)] for pair in range(pairs)])
        u = jnp.einsum("pxr,pxj->prj", x, g, preferred_element_type=F32)
        y = jnp.einsum("kx,pxj->pkj", closing, turn_halves(u, cosine, sine, first), preferred_element_type=F32)
        y = y.astype(BF16).reshape(pairs, second, 2, first).transpose(1, 3, 0, 2)
        return y.reshape(devices, here // span, span, channels).transpose(0, 1, 3, 2)
    low = second // devices
    whole = lambda step: (0, 0)
    return pl.pallas_call(
        functools.partial(transform_kernel, first),
        grid=(channels // STEP,),
        in_specs=[
            pl.BlockSpec((devices, STEP, here), lambda step: (0, step, 0)),
            pl.BlockSpec((2, 2 * first, 4 * first), lambda step: (0, 0, 0)),
            pl.BlockSpec((second, first), whole),
            pl.BlockSpec((second, first), whole),
            pl.BlockSpec((second, 2 * second), whole),
        ],
        out_specs=pl.BlockSpec((devices, low, STEP, first), lambda step: (0, 0, step, 0)),
        out_shape=jax.ShapeDtypeStruct((devices, low, channels, first), BF16),
        scratch_shapes=[
            pltpu.VMEM((here // LANES, devices * STEP, LANES), F32),
            pltpu.VMEM((second * STEP, first), F32),
        ],
        compiler_params=pltpu.CompilerParams(dimension_semantics=("arbitrary",)),
        cost_estimate=pl.CostEstimate(
            flops=channels * second * first * 8 * (first + second), bytes_accessed=4 * x.size, transcendentals=0
        ),
    )(x, g, cosine, sine, closing)


def fits(channels, here, first, devices):
    return first == LANES and channels % STEP == 0 and devices % 16 == 0 and here % (2 * first) == 0


def closing_kernel(r_ref, w_ref, gate_ref, *rest):
    out_ref = rest[-1]
    mixed = w_ref.shape[0]
    span = r_ref.shape[3]
    left = jnp.concatenate([r_ref[:, low].reshape(mixed, span) for low in range(r_ref.shape[1])], axis=1)
    mapped = lax.dot_general(left, w_ref[...], (((0,), (0,)), ((), ())), preferred_element_type=F32)
    out_ref[0] = (gate_ref[0].astype(F32) * mapped).astype(BF16)


def close(seq, returned, ordered, gate_value, so_far):
    devices, lows, channels, span = returned.shape
    seqs, here, width = gate_value.shape
    mixed = ordered.shape[0]
    many = 2
    block = pl.BlockSpec((1, many * span, width), lambda step: (seq, step, 0))
    operands = [returned, ordered, gate_value]
    in_specs = [
        pl.BlockSpec((devices, many, channels, span), lambda step: (0, step, 0, 0)),
        pl.BlockSpec((mixed, width), lambda step: (0, 0)),
        block,
    ]
    if so_far is not None:
        operands.append(so_far)
        in_specs.append(pl.BlockSpec(memory_space=pl.ANY))
    return pl.pallas_call(
        closing_kernel,
        grid=(lows // many,),
        in_specs=in_specs,
        out_specs=block,
        out_shape=jax.ShapeDtypeStruct((seqs, here, width), BF16),
        input_output_aliases={} if so_far is None else {3: 0},
        compiler_params=pltpu.CompilerParams(dimension_semantics=("arbitrary",)),
        cost_estimate=pl.CostEstimate(
            flops=2 * here * mixed * width, bytes_accessed=2 * (here * mixed + mixed * width + 2 * here * width),
            transcendentals=0,
        ),
    )(*operands)


def local(devices, tokens, norm_gain, mix_weight, gate_weight, out_weight):
    seqs, here, width = tokens.shape
    length = here * devices
    mixed = mix_weight.shape[1]
    groups = mixed // GROUP_DIM
    channels = mixed // devices
    first = max(GROUP_DIM, devices)
    span = min(first, here)

    mix = jnp.einsum(
        "dgj,jk->dgk", mix_weight.reshape(width, groups, GROUP_DIM), jnp.asarray(channel_table(), BF16),
        preferred_element_type=F32,
    ).astype(BF16).reshape(width, mixed)

    def norm(x):
        widened = x.astype(F32)
        inverse_rms = lax.rsqrt(jnp.mean(widened * widened, axis=-1, keepdims=True) + 1e-06)
        return (widened * inverse_rms * norm_gain).astype(BF16)

    def exchange(x):
        return lax.all_to_all(x, AXES, split_axis=0, concat_axis=0, tiled=True)

    lone_here = lax.axis_index(AXES) * (channels // 2) % HALF == 0
    transform = functools.partial(
        position_transform, lone_here=lone_here, devices=devices, length=length, first=first
    )
    arrived = []
    for seq in range(seqs):
        columns = lax.dot_general(
            mix, norm(tokens[seq]), (((0,), (1,)), ((), ())), preferred_element_type=F32
        ).astype(BF16).reshape(devices, channels, here)
        if seq:
            columns, arrived[-1] = lax.optimization_barrier((columns, arrived[-1]))
        arrived.append(exchange(columns))

    gate_value = jax.nn.sigmoid(jnp.dot(norm(tokens), gate_weight, preferred_element_type=F32)).astype(BF16)
    ordered = jnp.einsum(
        "ij,gjd->gid", jnp.asarray(channel_order(), BF16), out_weight.reshape(groups, GROUP_DIM, width),
        preferred_element_type=F32,
    ).astype(BF16).reshape(mixed, width)
    gate_value, ordered, arrived[-1] = lax.optimization_barrier((gate_value, ordered, arrived[-1]))

    returned = []
    for seq in range(seqs):
        spectra = transform(arrived[seq])
        if seq:
            spectra, returned[-1] = lax.optimization_barrier((spectra, returned[-1]))
        returned.append(exchange(spectra))

    if fits(channels, here, first, devices):
        gated = None
        for seq in range(seqs):
            gated = close(seq, returned[seq], ordered, gate_value, gated)
        return gated
    spectral = jnp.stack(returned).transpose(0, 2, 4, 1, 3).reshape(seqs, here, mixed)
    mapped = jnp.dot(spectral, ordered, preferred_element_type=F32)
    return (gate_value * mapped).astype(BF16)


def solution(mesh):
    in_specs = (P(None, AXES, None), P(), P(), P(), P())
    devices = mesh.shape["row"] * mesh.shape["col"]
    body = functools.partial(local, devices)
    return jax.shard_map(body, mesh=mesh, in_specs=in_specs, out_specs=P(None, AXES, None), check_vma=False)
```

profile of v0, /device:TPU:0, one launch (start us, length us, event | category | flops | bytes accessed | tf_op | source)
XLA Modules:
  0.0 240.3 jit_solution(2586095227350989311)
XLA Ops:
  0.0 4.5 %fusion.6 = (f32[1024]{0:T(1024)S(1)}, f32[1024]{0:T(1024)S(1)}) fusion(bf16[2,1024,2048]{2,1,0:T(8,128)(2,1)} %param.17), kind=kLoop, calls=%fused_computation.13 | loop fusion | flops 12580864 | bytes 8396800 | tf_op jit(solution)/shard_map/reduce_sum | solution.py:211
  4.5 0.3 copy-done.1
  4.8 1.3 fusion.31
  6.2 1.5 slice-done.1
  7.6 6.2 %fusion.39 = bf16[1024,1024]{1,0:T(8,128)(2,1)} fusion(bf16[2048,1024]{0,1:T(8,128)(2,1)S(1)} %bitcast.47, f32[1024]{0:T(1024)S(1)} %get-tuple-element.21, f32[2048]{0:T(1024)S(1)} %copy-done.11, bf16[2,1024,2048]{2,1,0:T(8,128)(2,1)S(1)} %bitcast.45), kind=kOutput, calls=%fused_computation.36 | convolution fusion | flops 4304404480 | bytes 10498048 | tf_op jit(solution)/shard_map/dot_general | solution.py:223
  13.8 7.3 %all-to-all-start = ((bf16[32,32,1024]{2,1,0:T(8,128)(2,1)}), bf16[32,32,1024]{2,1,0:T(8,128)(2,1)S(1)}, u32[]{:S(2)}, u32[]{:S(2)}) async-start(bf16[32,32,1024]{2,1,0:T(8,128)(2,1)} %bitcast.50), calls=%async_computation | async-start | bytes 4194304 | tf_op jit(solution)/shard_map/all_to_all | solution.py:215
  21.2 9.5 %fusion.36 = bf16[1024,1024]{1,0:T(8,128)(2,1)} fusion(bf16[2048,1024]{0,1:T(8,128)(2,1)} %bitcast.48, f32[2048]{0:T(1024)S(1)} %copy-done.11, f32[1024]{0:T(1024)S(1)} %get-tuple-element.22, bf16[2,1024,2048]{2,1,0:T(8,128)(2,1)} %param.17), kind=kOutput, calls=%fused_computation.35 | convolution fusion | flops 4304404480 | bytes 10498048 | tf_op jit(solution)/shard_map/dot_general | solution.py:223
  30.7 39.2 %all-to-all-done.x_ref = bf16[32,32,1024]{2,1,0:T(8,128)(2,1)S(1)} async-done(((bf16[32,32,1024]{2,1,0:T(8,128)(2,1)}), bf16[32,32,1024]{2,1,0:T(8,128)(2,1)S(1)}, u32[]{:S(2)}, u32[]{:S(2)}) %all-to-all-start) | async-done | bytes 2097184 | tf_op jit(solution)/shard_map/all_to_all | solution.py:215
  69.9 1.3 copy-done.5
  71.2 4.2 %all-to-all-start.1 = ((bf16[32,32,1024]{2,1,0:T(8,128)(2,1)}), bf16[32,32,1024]{2,1,0:T(8,128)(2,1)S(1)}, u32[]{:S(2)}, u32[]{:S(2)}) async-start(bf16[32,32,1024]{2,1,0:T(8,128)(2,1)} %bitcast.49), calls=%async_computation.1 | async-start | bytes 4194304 | tf_op jit(solution)/shard_map/all_to_all | solution.py:215
  75.5 0.8 pad_maximum_fusion.g_ref
  76.3 5.6 %fusion = f32[2,1024]{1,0:T(2,128)S(1)} fusion(bf16[2,1024,2048]{2,1,0:T(8,128)(2,1)} %param.17), kind=kLoop, calls=%fused_computation.2 | loop fusion | flops 12580864 | bytes 8396800 | tf_op jit(solution)/shard_map/reduce_sum | solution.py:211
  82.0 3.2 %convolution_convert_fusion = bf16[128,8,2048]{2,0,1:T(8,128)(2,1)} fusion(bf16[128,128,1]{1,0,2:T(8,128)(2,1)S(1)} %copy-done.9, bf16[8,128,2048]{2,1,0:T(8,128)(2,1)S(1)} %bitcast.46), kind=kOutput, calls=%fused_computation.32 | convolution fusion | flops 538968064 | bytes 8421376 | tf_op jit(solution)/shard_map/ij,gjd->gid/dot_general | solution.py:231
  85.2 6.8 %shard_map.164 = bf16[32,8,32,128]{3,2,1,0:T(8,128)(2,1)} custom-call(bf16[32,32,1024]{2,1,0:T(8,128)(2,1)} %copy-done.5, bf16[2,256,512]{2,1,0:T(8,128)(2,1)} %pad_maximum_fusion.g_ref, f32[256,128]{1,0:T(8,128)} %constant.58.clone.cos_ref, f32[256,128]{1,0:T(8,128)} %constant.59.clone.sin_ref, bf16[256,512]{1,0:T(8,128)(2,1)} %constant.60.clone.close_ref), custom_call_target="tpu_custom_call" | custom-call | flops 3221225472 | bytes 4194304 | tf_op jit(solution)/shard_map/pallas_call | solution.py:129
  92.1 31.9 %all-to-all-done.1.x_ref = bf16[32,32,1024]{2,1,0:T(8,128)(2,1)S(1)} async-done(((bf16[32,32,1024]{2,1,0:T(8,128)(2,1)}), bf16[32,32,1024]{2,1,0:T(8,128)(2,1)S(1)}, u32[]{:S(2)}, u32[]{:S(2)}) %all-to-all-start.1) | async-done | bytes 2097184 | tf_op jit(solution)/shard_map/all_to_all | solution.py:215
  123.9 1.3 copy-done.4
  125.3 4.0 %all-to-all-start.2 = ((bf16[32,8,32,128]{3,2,1,0:T(8,128)(2,1)}), bf16[32,8,32,128]{3,2,1,0:T(8,128)(2,1)S(1)}, u32[]{:S(2)}, u32[]{:S(2)}) async-start(bf16[32,8,32,128]{3,2,1,0:T(8,128)(2,1)} %shard_map.164), calls=%async_computation.2 | async-start | bytes 4194304 | tf_op jit(solution)/shard_map/all_to_all | solution.py:215
  129.3 26.3 %divide_convert_fusion.gate_ref = bf16[2,1024,2048]{2,1,0:T(8,128)(2,1)} fusion(bf16[2048,2048]{1,0:T(8,128)(2,1)} %param.20, bf16[2,1024,2048]{2,1,0:T(8,128)(2,1)} %param.17, f32[2048]{0:T(1024)S(1)} %copy-done.11, f32[2,1024]{1,0:T(2,128)S(1)} %add_rsqrt_fusion), kind=kOutput, calls=%fused_computation.5 | convolution fusion | flops 17213423616 | bytes 25182208 | tf_op jit(solution)/shard_map/dot_general | solution.py:230
  155.5 6.8 %shard_map.163 = bf16[32,8,32,128]{3,2,1,0:T(8,128)(2,1)} custom-call(bf16[32,32,1024]{2,1,0:T(8,128)(2,1)} %copy-done.4, bf16[2,256,512]{2,1,0:T(8,128)(2,1)} %pad_maximum_fusion.g_ref, f32[256,128]{1,0:T(8,128)} %constant.58.clone.cos_ref, f32[256,128]{1,0:T(8,128)} %constant.59.clone.sin_ref, bf16[256,512]{1,0:T(8,128)(2,1)} %constant.60.clone.close_ref), custom_call_target="tpu_custom_call" | custom-call | flops 3221225472 | bytes 4194304 | tf_op jit(solution)/shard_map/pallas_call | solution.py:129
  162.4 15.6 %all-to-all-done.2.r_ref = bf16[32,8,32,128]{3,2,1,0:T(8,128)(2,1)S(1)} async-done(((bf16[32,8,32,128]{3,2,1,0:T(8,128)(2,1)}), bf16[32,8,32,128]{3,2,1,0:T(8,128)(2,1)S(1)}, u32[]{:S(2)}, u32[]{:S(2)}) %all-to-all-start.2) | async-done | bytes 2097184 | tf_op jit(solution)/shard_map/all_to_all | solution.py:215
  178.0 4.1 %all-to-all-start.3 = ((bf16[32,8,32,128]{3,2,1,0:T(8,128)(2,1)}), bf16[32,8,32,128]{3,2,1,0:T(8,128)(2,1)}, u32[]{:S(2)}, u32[]{:S(2)}) async-start(bf16[32,8,32,128]{3,2,1,0:T(8,128)(2,1)} %shard_map.163), calls=%async_computation.3 | async-start | bytes 4194304 | tf_op jit(solution)/shard_map/all_to_all | solution.py:215
  182.2 9.4 %shard_map.165.rest_0_ = bf16[2,1024,2048]{2,1,0:T(8,128)(2,1)} custom-call(bf16[32,8,32,128]{3,2,1,0:T(8,128)(2,1)} %copy-done, bf16[1024,2048]{1,0:T(8,128)(2,1)} %bitcast.42, bf16[2,1024,2048]{2,1,0:T(8,128)(2,1)} %divide_convert_fusion.gate_ref), custom_call_target="tpu_custom_call" | custom-call | flops 4294967296 | bytes 14680064 | tf_op jit(solution)/shard_map/pallas_call | solution.py:180
  191.6 39.2 %all-to-all-done.3.r_ref = bf16[32,8,32,128]{3,2,1,0:T(8,128)(2,1)} async-done(((bf16[32,8,32,128]{3,2,1,0:T(8,128)(2,1)}), bf16[32,8,32,128]{3,2,1,0:T(8,128)(2,1)}, u32[]{:S(2)}, u32[]{:S(2)}) %all-to-all-start.3) | async-done | bytes 2097184 | tf_op jit(solution)/shard_map/all_to_all | solution.py:215
  230.8 9.4 %shard_map.166 = bf16[2,1024,2048]{2,1,0:T(8,128)(2,1)} custom-call(bf16[32,8,32,128]{3,2,1,0:T(8,128)(2,1)} %all-to-all-done.3.r_ref, bf16[1024,2048]{1,0:T(8,128)(2,1)} %bitcast.43, bf16[2,1024,2048]{2,1,0:T(8,128)(2,1)} %divide_convert_fusion.gate_ref, bf16[2,1024,2048]{2,1,0:T(8,128)(2,1)} %shard_map.165.rest_0_), custom_call_target="tpu_custom_call", output_to_operand_aliasing={{}: (3, {})} | custom-call | flops 4294967296 | bytes 14680064 | tf_op jit(solution)/shard_map/pallas_call | solution.py:180
  (28 shorter events, 0.1 us)
Async XLA Ops:
  0.0 4.5 %copy-start.10 = (bf16[128,128,1]{0,1,2:T(8,128)(2,1)S(1)}, bf16[128,128,1]{0,1,2:T(8,128)(2,1)}, u32[]{:S(2)}) copy-start(bf16[128,128,1]{0,1,2:T(8,128)(2,1)} %constant.63) | copy-start | bytes 98308
  0.0 6.1 %slice-start = ((s8[8388608]{0:T(1024)(128)(4,1)}), s8[4194304]{0:T(1024)(128)(4,1)S(1)}, s32[]{:S(2)}) async-start(s8[8388608]{0:T(1024)(128)(4,1)} %bitcast.44), calls=%async_computation.4 | async-start | bytes 8388608
  0.0 4.8 %copy-start.1 = (bf16[2048,1024]{1,0:T(8,128)(2,1)S(1)}, bf16[2048,1024]{1,0:T(8,128)(2,1)}, u32[]{:S(2)}) copy-start(bf16[2048,1024]{1,0:T(8,128)(2,1)} %param.19) | copy-start | bytes 12582916
  0.0 6.1 %copy-start.11 = (f32[2048]{0:T(1024)S(1)}, f32[2048]{0:T(1024)}, u32[]{:S(2)}) copy-start(f32[2048]{0:T(1024)} %param.18) | copy-start | bytes 24580
  4.8 2.8 %slice-start.1 = ((s8[8388608]{0:T(1024)(128)(4,1)}), s8[4194304]{0:T(1024)(128)(4,1)S(1)}, s32[]{:S(2)}) async-start(s8[8388608]{0:T(1024)(128)(4,1)} %bitcast.44), calls=%async_computation.5 | async-start | bytes 8388608
  6.1 7.7 %copy-start.3 = (bf16[128,2048,8]{1,0,2:T(8,128)(2,1)}, bf16[128,2048,8]{1,0,2:T(8,128)(2,1)S(1)}, u32[]{:S(2)}) copy-start(bf16[128,2048,8]{1,0,2:T(8,128)(2,1)S(1)} %fusion.31) | copy-start | bytes 12582916
  13.8 56.0 %all-to-all-start = ((bf16[32,32,1024]{2,1,0:T(8,128)(2,1)}), bf16[32,32,1024]{2,1,0:T(8,128)(2,1)S(1)}, u32[]{:S(2)}, u32[]{:S(2)}) async-start(bf16[32,32,1024]{2,1,0:T(8,128)(2,1)} %bitcast.50), calls=%async_computation | async-start | bytes 4194304 | tf_op jit(solution)/shard_map/all_to_all | solution.py:215
  21.2 54.3 %copy-start.7 = (bf16[256,512]{1,0:T(8,128)(2,1)S(1)}, bf16[256,512]{1,0:T(8,128)(2,1)}, u32[]{:S(2)}) copy-start(bf16[256,512]{1,0:T(8,128)(2,1)} %constant.57.clone) | copy-start | bytes 786436
  21.2 54.3 %copy-start.8 = (bf16[256,512]{1,0:T(8,128)(2,1)S(1)}, bf16[256,512]{1,0:T(8,128)(2,1)}, u32[]{:S(2)}) copy-start(bf16[256,512]{1,0:T(8,128)(2,1)} %constant.56.clone) | copy-start | bytes 786436
  21.2 54.3 %copy-start.6 = (bf16[1,256,512]{2,1,0:T(8,128)(2,1)S(1)}, bf16[1,256,512]{2,1,0:T(8,128)(2,1)}, u32[]{:S(2)}) copy-start(bf16[1,256,512]{2,1,0:T(8,128)(2,1)} %constant.61) | copy-start | bytes 786436
  30.7 51.3 %copy-start.9 = (bf16[128,128,1]{1,0,2:T(8,128)(2,1)S(1)}, bf16[128,128,1]{1,0,2:T(8,128)(2,1)}, u32[]{:S(2)}) copy-start(bf16[128,128,1]{1,0,2:T(8,128)(2,1)} %constant.62) | copy-start | bytes 98308
  69.9 1.3 copy-start.5
  71.2 52.7 %all-to-all-start.1 = ((bf16[32,32,1024]{2,1,0:T(8,128)(2,1)}), bf16[32,32,1024]{2,1,0:T(8,128)(2,1)S(1)}, u32[]{:S(2)}, u32[]{:S(2)}) async-start(bf16[32,32,1024]{2,1,0:T(8,128)(2,1)} %bitcast.49), calls=%async_computation.1 | async-start | bytes 4194304 | tf_op jit(solution)/shard_map/all_to_all | solution.py:215
  75.4 6.6 %copy-start.2 = (bf16[1024,2048]{1,0:T(8,128)(2,1)S(1)}, bf16[1024,2048]{1,0:T(8,128)(2,1)}, u32[]{:S(2)}) copy-start(bf16[1024,2048]{1,0:T(8,128)(2,1)} %param.21) | copy-start | bytes 12582916
  123.9 1.3 copy-start.4
  125.3 52.7 %all-to-all-start.2 = ((bf16[32,8,32,128]{3,2,1,0:T(8,128)(2,1)}), bf16[32,8,32,128]{3,2,1,0:T(8,128)(2,1)S(1)}, u32[]{:S(2)}, u32[]{:S(2)}) async-start(bf16[32,8,32,128]{3,2,1,0:T(8,128)(2,1)} %shard_map.164), calls=%async_computation.2 | async-start | bytes 4194304 | tf_op jit(solution)/shard_map/all_to_all | solution.py:215
  178.0 4.2 %copy-start = (bf16[32,8,32,128]{3,2,1,0:T(8,128)(2,1)}, bf16[32,8,32,128]{3,2,1,0:T(8,128)(2,1)S(1)}, u32[]{:S(2)}) copy-start(bf16[32,8,32,128]{3,2,1,0:T(8,128)(2,1)S(1)} %all-to-all-done.2.r_ref) | copy-start | bytes 6291460
  178.0 52.8 %all-to-all-start.3 = ((bf16[32,8,32,128]{3,2,1,0:T(8,128)(2,1)}), bf16[32,8,32,128]{3,2,1,0:T(8,128)(2,1)}, u32[]{:S(2)}, u32[]{:S(2)}) async-start(bf16[32,8,32,128]{3,2,1,0:T(8,128)(2,1)} %shard_map.163), calls=%async_computation.3 | async-start | bytes 4194304 | tf_op jit(solution)/shard_map/all_to_all | solution.py:215
where the time goes:
time: 241 us; the launch traced here: 240 us
  waiting for transfers between devices  126 us (52%)
  matrix products  46.5 us (19%)
  Pallas kernels  32.5 us (13%)
  starting transfers between devices  19.7 us (8%)
  other arithmetic  11 us (5%)
  local copies, waits for them, and re-layouts  4.42 us (2%)
    all_to_all x4, waiting for transfers between devices, exchange(): return lax.all_to_all(x, AXES, split_axis=0, concat_axis=0, tiled=True)  126 us
    dot_general x1, matrix products, local(): jnp.dot(norm(tokens), gate_weight, preferred_element_type=F32)  26.3 us
    all_to_all x4, starting transfers between devices, exchange(): return lax.all_to_all(x, AXES, split_axis=0, concat_axis=0, tiled=True)  19.7 us
    pallas_call x2, Pallas kernels, close(): pl.pallas_call(closing_kernel, grid=(lows // many,), in_specs=in_specs, o...  18.9 us
    dot_general x2, matrix products, local(): lax.dot_general(mix, norm(tokens[seq]), (((0,), (1,)), ((), ())), preferr...  15.7 us
    pallas_call x2, Pallas kernels, position_transform(): pl.pallas_call(functools.partial(transform_kernel, first), grid=(channels...  13.7 us
    reduce_sum x2, other arithmetic, norm(): jnp.mean(widened * widened, axis=-1, keepdims=True) + 1e-06  10.1 us
  transfers between devices with their start and end apart: 4, of which 4 were waited for; matrix products, arithmetic and copies ran while one was open for 19% of the time, Pallas kernels for 10%

commit v1 on v0

v1 whole, which is shorter than its diff:
```python
import functools
import math

import jax
import jax.numpy as jnp
import numpy as np
from jax import lax
from jax.experimental import pallas as pl
from jax.experimental.pallas import tpu as pltpu
from jax.sharding import PartitionSpec as P

GROUP_DIM = 128
HALF = GROUP_DIM // 2
BF16 = jnp.bfloat16
F32 = jnp.float32
AXES = ("row", "col")
LANES = 128
BLOCK = 16
WIDE = 256
NT = (((1,), (1,)), ((), ()))
MESH = pl.DeviceIdType.MESH


def angles(left, right, period):
    return (np.outer(left, right) % period) * (2.0 * math.pi / period)


def channel_table():
    phase = angles(np.arange(GROUP_DIM), np.arange(HALF), GROUP_DIM)
    table = np.stack([np.cos(phase), np.sin(phase)], axis=-1)
    table[:, 0, 1] = np.cos(math.pi * np.arange(GROUP_DIM))
    return table.reshape(GROUP_DIM, GROUP_DIM) * GROUP_DIM ** -0.5


def channel_order():
    order = np.zeros((HALF, 2), np.int64)
    order[:, 0] = np.arange(HALF)
    order[:, 1] = GROUP_DIM - np.arange(HALF)
    order[0, 1] = HALF
    pick = np.zeros((GROUP_DIM, GROUP_DIM))
    pick[np.arange(GROUP_DIM), order.reshape(-1)] = 1.0
    return pick


def position_tables(devices, length, first):
    second, fold = length // first, first // devices
    phase = angles(np.arange(first), np.arange(first), first)
    cosine, sine = np.cos(phase), np.sin(phase)
    zero = np.zeros_like(cosine)
    from_left = np.concatenate([cosine, sine, cosine, sine], axis=1)
    from_right = np.concatenate([-sine, cosine, sine, -cosine], axis=1)
    lone_left = np.concatenate([cosine, sine, zero, zero], axis=1)
    lone_right = np.concatenate([zero, zero, cosine, sine], axis=1)

    def interleave(left, right):
        pair = np.stack([left, right]).reshape(2, devices, fold, -1).transpose(0, 2, 1, 3)
        return pair.reshape(2 * first, 4 * first)

    turn = angles(np.arange(second), np.arange(first), length)
    last = angles(np.arange(second), np.arange(second), second)
    closing = np.concatenate([np.cos(last), -np.sin(last)], axis=1) * length ** -0.5
    return (
        interleave(from_left, from_right),
        interleave(lone_left, lone_right),
        np.cos(turn),
        np.sin(turn),
        closing,
    )


def turn_halves(u, cosine, sine, first):
    halves = []
    for half in range(2):
        real = u[..., 2 * half * first : (2 * half + 1) * first]
        imag = u[..., (2 * half + 1) * first : (2 * half + 2) * first]
        halves.append(
            jnp.concatenate(
                [(real * cosine - imag * sine).astype(BF16), (real * sine + imag * cosine).astype(BF16)], axis=-2
            )
        )
    return jnp.concatenate(halves, axis=-1)


def position_transform(x, lone_here, devices, length, first):
    _, channels, here = x.shape
    second, fold = length // first, first // devices
    normal, lone, cosine, sine, closing = position_tables(devices, length, first)
    normal, lone = jnp.asarray(normal, BF16), jnp.asarray(lone, BF16)
    cosine, sine, closing = jnp.asarray(cosine, F32), jnp.asarray(sine, F32), jnp.asarray(closing, BF16)
    g = jnp.stack([jnp.where(lone_here, lone, normal), normal])
    pairs, span = channels // 2, min(first, here)
    x = x.reshape(devices, pairs, 2, fold, second).transpose(1, 2, 3, 0, 4).reshape(pairs, 2 * first, second)
    g = jnp.stack([g[min(pair, 1)] for pair in range(pairs)])
    u = jnp.einsum("pxr,pxj->prj", x, g, preferred_element_type=F32)
    y = jnp.einsum("kx,pxj->pkj", closing, turn_halves(u, cosine, sine, first), preferred_element_type=F32)
    y = y.astype(BF16).reshape(pairs, second, 2, first).transpose(1, 3, 0, 2)
    return y.reshape(devices, here // span, span, channels).transpose(0, 1, 3, 2)


def plain(devices, tokens, norm_gain, mix_weight, gate_weight, out_weight):
    seqs, here, width = tokens.shape
    length = here * devices
    mixed = mix_weight.shape[1]
    groups = mixed // GROUP_DIM
    channels = mixed // devices
    first = max(GROUP_DIM, devices)
    mix = jnp.einsum(
        "dgj,jk->dgk", mix_weight.reshape(width, groups, GROUP_DIM), jnp.asarray(channel_table(), BF16),
        preferred_element_type=F32,
    ).astype(BF16).reshape(width, mixed)
    ordered = jnp.einsum(
        "ij,gjd->gid", jnp.asarray(channel_order(), BF16), out_weight.reshape(groups, GROUP_DIM, width),
        preferred_element_type=F32,
    ).astype(BF16).reshape(mixed, width)
    widened = tokens.astype(F32)
    inverse_rms = lax.rsqrt(jnp.mean(widened * widened, axis=-1, keepdims=True) + 1e-06)
    normed = (widened * inverse_rms * norm_gain).astype(BF16)
    gate_value = jax.nn.sigmoid(jnp.dot(normed, gate_weight, preferred_element_type=F32)).astype(BF16)
    lone_here = lax.axis_index(AXES) * (channels // 2) % HALF == 0

    def exchange(x):
        return lax.all_to_all(x, AXES, split_axis=0, concat_axis=0, tiled=True)

    returned = []
    for seq in range(seqs):
        columns = lax.dot_general(
            mix, normed[seq], (((0,), (1,)), ((), ())), preferred_element_type=F32
        ).astype(BF16).reshape(devices, channels, here)
        returned.append(exchange(position_transform(exchange(columns), lone_here, devices, length, first)))
    spectral = jnp.stack(returned).transpose(0, 2, 4, 1, 3).reshape(seqs, here, mixed)
    mapped = jnp.dot(spectral, ordered, preferred_element_type=F32)
    return (gate_value * mapped).astype(BF16)


def mixer_kernel(
    rows, cols, tokens, gain_in, mix_in, gate_in, out_in, table_in, order_in, eye_in, spread_in, cos_in, sin_in,
    close_in, result, token_v, normed, mix_v, gate_v, out_v, gain_v, table_v, order_v, eye_v, spread_v, cos_v, sin_v,
    close_v, send_f, recv_f, send_r, recv_r, rows_in, rows_out, left_v, stage, load_sem, token_sem, stage_sem,
    send_f_sem, recv_f_sem, send_r_sem, recv_r_sem,
):
    devices = rows * cols
    row, col = lax.axis_index("row"), lax.axis_index("col")
    me = row * cols + col
    parts, tile, width = stage.shape[0], token_v.shape[1], token_v.shape[2]
    tiles = send_f.shape[0]
    seqs = tokens.shape[0]
    per_seq = tiles // seqs
    channels = send_f.shape[2]
    mixed = devices * channels
    first, second = cos_v.shape
    lows = send_r.shape[2]
    per_group = GROUP_DIM // channels

    barrier = pltpu.get_barrier_semaphore()

    def partner(k):
        there_row, there_col = lax.rem(row + lax.rem(k, rows), rows), lax.rem(col + k // rows, cols)
        return there_row, there_col, there_row * cols + there_col

    def greet(k, carry):
        there_row, there_col, _ = partner(k)
        pl.semaphore_signal(barrier, inc=1, device_id=(there_row, there_col), device_id_type=MESH)
        return carry

    def token_load(i):
        slot = lax.rem(i, 2)
        start = pl.multiple_of(lax.rem(i, per_seq) * tile, tile)
        return pltpu.make_async_copy(
            tokens.at[i // per_seq, pl.ds(start, tile), :], token_v.at[slot], token_sem.at[slot]
        )

    loads = [
        pltpu.make_async_copy(here, there, load_sem.at[at])
        for at, (here, there) in enumerate([
            (gain_in, gain_v), (mix_in, mix_v), (table_in, table_v), (spread_in, spread_v), (cos_in, cos_v),
            (sin_in, sin_v), (close_in, close_v), (gate_in, gate_v), (out_in, out_v), (order_in, order_v),
            (eye_in, eye_v),
        ])
    ]
    token_load(0).start()
    for load in loads[:3]:
        load.start()
    lax.fori_loop(1, devices, greet, 0)

    def norm(i):
        slot = lax.rem(i, 2)
        token_load(i).wait()

        def strip(r, carry):
            at = pl.ds(pl.multiple_of(r * 32, 32), 32)
            widened = token_v[slot, at, :].astype(F32)
            inverse_rms = lax.rsqrt(jnp.mean(widened * widened, axis=-1, keepdims=True) + 1e-06)
            normed[i + 1, at, :] = (widened * inverse_rms * gain_v[...]).astype(BF16)
            return carry

        lax.fori_loop(0, tile // 32, strip, 0)

    def send(send_ref, recv_ref, send_sem, recv_sem, i):
        def one(k, carry):
            there_row, there_col, there = partner(k)
            pltpu.make_async_remote_copy(
                src_ref=send_ref.at[i, there], dst_ref=recv_ref.at[i, me], send_sem=send_sem.at[i],
                recv_sem=recv_sem.at[i], device_id=(there_row, there_col), device_id_type=MESH,
            ).start()
            return carry

        recv_ref[i, me] = send_ref[i, me]
        lax.fori_loop(1, devices, one, 0)

    def await_all(ref, sem, i):
        others = ref.at[i, pl.ds(0, devices - 1)]
        pltpu.make_async_copy(others, others, sem.at[i]).wait()

    loads[0].wait()
    norm(0)
    token_load(1).start()
    for load in loads[3:]:
        load.start()
    loads[1].wait()
    loads[2].wait()
    pl.semaphore_wait(barrier, devices - 1)

    def forward(i, carry):
        def columns(n, carry):
            at = pl.ds(pl.multiple_of(n * WIDE, WIDE), WIDE)
            mixed_in = jnp.dot(normed[i + 1], mix_v[:, at], preferred_element_type=F32).astype(BF16)
            for part in range(WIDE // GROUP_DIM):
                turned = lax.dot_general(
                    table_v[...], mixed_in[:, part * GROUP_DIM : (part + 1) * GROUP_DIM], NT,
                    preferred_element_type=F32,
                ).astype(BF16)
                owner = (n * (WIDE // GROUP_DIM) + part) * per_group
                send_f[i, pl.ds(owner, per_group)] = turned.reshape(per_group, channels, tile)
            return carry

        lax.fori_loop(0, mixed // WIDE, columns, 0)
        send(send_f, recv_f, send_f_sem, recv_f_sem, i)

        @pl.when(i + 1 < tiles)
        def _():
            @pl.when(i + 2 < tiles)
            def _():
                token_load(i + 2).start()

            norm(i + 1)

        return carry

    lax.fori_loop(0, tiles, forward, 0)
    for load in loads[3:]:
        load.wait()

    for group in range(mixed // GROUP_DIM):
        at = pl.ds(group * GROUP_DIM, GROUP_DIM)
        out_v[at, :] = jnp.dot(order_v[...], out_v[at, :], preferred_element_type=F32).astype(BF16)

    def transform(seq):
        def block(b, carry):
            these = pl.ds(pl.multiple_of(b * BLOCK, BLOCK), BLOCK)
            for t in range(per_seq):
                for half in range(tile // LANES):
                    rows_in[t * (tile // LANES) + half] = (
                        recv_f[seq * per_seq + t, :, these, half * LANES : (half + 1) * LANES]
                        .astype(F32).reshape(devices * BLOCK, LANES)
                    )
            for pair in range(BLOCK // 2):
                picked = []
                for column in range(2):
                    for t in range(per_seq):
                        at = pl.ds(2 * pair + column, devices, stride=BLOCK)
                        picked.append(
                            jnp.concatenate(
                                [rows_in[t * (tile // LANES) + half, at, :] for half in range(tile // LANES)], axis=1
                            ).astype(BF16)
                        )
                x = jnp.concatenate(picked, axis=0)
                if pair == 0:
                    lone = jnp.logical_and(b == 0, lax.rem(me, per_group) == 0)
                    spread = spread_v[jnp.where(lone, 0, 1)]
                else:
                    spread = spread_v[1]
                u = jnp.dot(spread, x, preferred_element_type=F32)
                cosine, sine = cos_v[...], sin_v[...]
                halves = []
                for half in range(2):
                    real = u[2 * half * first : (2 * half + 1) * first]
                    imag = u[(2 * half + 1) * first : (2 * half + 2) * first]
                    halves.append(
                        jnp.concatenate(
                            [(real * cosine - imag * sine).astype(BF16), (real * sine + imag * cosine).astype(BF16)],
                            axis=1,
                        )
                    )
                turned = jnp.concatenate(halves, axis=0)
                y = lax.dot_general(close_v[...], turned, NT, preferred_element_type=F32)
                for half in range(2):
                    rows_out[pl.ds(2 * pair + half, second, stride=BLOCK), :] = y[:, half * first : (half + 1) * first]

            def leave(there, carry):
                span = second // devices * BLOCK
                out = rows_out[pl.ds(pl.multiple_of(there * span, span), span), :].reshape(-1, BLOCK, LANES)
                for q in range(per_seq):
                    send_r[seq * per_seq + q, there, :, these, :] = out[q * lows : (q + 1) * lows].astype(BF16)
                return carry

            lax.fori_loop(0, devices, leave, 0)
            return carry

        lax.fori_loop(0, channels // BLOCK, block, 0)

    def middle(seq, carry):
        for t in range(per_seq):
            await_all(recv_f, recv_f_sem, seq * per_seq + t)
        transform(seq)
        for q in range(per_seq):
            send(send_r, recv_r, send_r_sem, recv_r_sem, seq * per_seq + q)

        def gate(at, carry):
            i, n = seq * per_seq + at // (width // WIDE), lax.rem(at, width // WIDE)
            these = pl.ds(pl.multiple_of(n * WIDE, WIDE), WIDE)
            logits = jnp.dot(normed[i + 1], gate_v[:, these], preferred_element_type=F32)
            normed[i, :, these] = jax.nn.sigmoid(logits).astype(BF16)
            return carry

        lax.fori_loop(0, per_seq * (width // WIDE), gate, 0)
        return carry

    lax.fori_loop(0, seqs, middle, 0)

    def put(j):
        slot = lax.rem(j, parts)
        start = pl.multiple_of(lax.rem(j, per_seq) * tile, tile)
        return pltpu.make_async_copy(
            stage.at[slot], result.at[j // per_seq, pl.ds(start, tile), :], stage_sem.at[slot]
        )

    def finish(j, carry):
        slot = lax.rem(j, parts)
        await_all(recv_r, recv_r_sem, j)

        @pl.when(j >= parts)
        def _():
            put(j - parts).wait()

        left = jnp.concatenate([recv_r[j, :, low].reshape(mixed, LANES) for low in range(lows)], axis=1)
        left_v[...] = lax.dot_general(eye_v[...], left, NT, preferred_element_type=F32).astype(BF16)

        def columns(n, carry):
            these = pl.ds(pl.multiple_of(n * WIDE, WIDE), WIDE)
            mapped = jnp.dot(left_v[...], out_v[:, these], preferred_element_type=F32)
            stage[slot, :, these] = (normed[j, :, these].astype(F32) * mapped).astype(BF16)
            return carry

        lax.fori_loop(0, width // WIDE, columns, 0)
        put(j).start()
        return carry

    lax.fori_loop(0, tiles, finish, 0)
    for j in range(tiles - parts, tiles):
        put(j).wait()
    for i in range(tiles):
        await_all(send_f, send_f_sem, i)
        await_all(send_r, send_r_sem, i)


def fused(rows, cols, tokens, norm_gain, mix_weight, gate_weight, out_weight):
    devices = rows * cols
    seqs, here, width = tokens.shape
    length = here * devices
    mixed = mix_weight.shape[1]
    channels = mixed // devices
    first = GROUP_DIM
    second = length // first
    tile = second
    tiles = seqs * here // tile
    lows = tile // first
    normal, lone, cosine, sine, closing = position_tables(devices, length, first)
    constants = [
        jnp.asarray(channel_table().T, BF16),
        jnp.asarray(channel_order(), BF16),
        jnp.eye(tile, dtype=BF16),
        jnp.asarray(np.stack([lone.T, normal.T]), BF16),
        jnp.asarray(cosine.T, F32),
        jnp.asarray(sine.T, F32),
        jnp.asarray(closing, BF16),
    ]
    operands = [tokens, norm_gain.reshape(1, width), mix_weight, gate_weight, out_weight, *constants]
    hbm = pl.BlockSpec(memory_space=pl.ANY)
    parts = 2
    scratch = [
        pltpu.VMEM((2, tile, width), BF16),
        pltpu.VMEM((tiles + 1, tile, width), BF16),
        pltpu.VMEM(mix_weight.shape, BF16),
        pltpu.VMEM(gate_weight.shape, BF16),
        pltpu.VMEM(out_weight.shape, BF16),
        pltpu.VMEM((1, width), F32),
        *[pltpu.VMEM(constant.shape, constant.dtype) for constant in constants],
        pltpu.VMEM((tiles, devices, channels, tile), BF16),
        pltpu.VMEM((tiles, devices, channels, tile), BF16),
        pltpu.VMEM((tiles, devices, lows, channels, first), BF16),
        pltpu.VMEM((tiles, devices, lows, channels, first), BF16),
        pltpu.VMEM((here // LANES, devices * BLOCK, LANES), F32),
        pltpu.VMEM((second * BLOCK, first), F32),
        pltpu.VMEM((tile, mixed), BF16),
        pltpu.VMEM((parts, tile, width), BF16),
        pltpu.SemaphoreType.DMA((4 + len(constants),)),
        pltpu.SemaphoreType.DMA((2,)),
        pltpu.SemaphoreType.DMA((parts,)),
        *[pltpu.SemaphoreType.DMA((tiles,)) for _ in range(4)],
    ]
    return pl.pallas_call(
        functools.partial(mixer_kernel, rows, cols),
        in_specs=[hbm] * len(operands),
        out_specs=hbm,
        out_shape=jax.ShapeDtypeStruct(tokens.shape, BF16),
        scratch_shapes=scratch,
        compiler_params=pltpu.CompilerParams(
            collective_id=0, has_side_effects=True, vmem_limit_bytes=60 * 2**20
        ),
        name="mixer",
    )(*operands)


def fits(devices, tokens, mix_weight):
    seqs, here, width = tokens.shape
    mixed = mix_weight.shape[1]
    second = here * devices // GROUP_DIM
    return (
        devices % 16 == 0
        and GROUP_DIM % devices == 0
        and mixed % (devices * BLOCK) == 0
        and second % WIDE == 0
        and here % second == 0
        and here // second == GROUP_DIM // devices
        and mixed % WIDE == 0
        and width % WIDE == 0
    )


def local(rows, cols, tokens, norm_gain, mix_weight, gate_weight, out_weight):
    args = (tokens, norm_gain, mix_weight, gate_weight, out_weight)
    if fits(rows * cols, tokens, mix_weight):
        return fused(rows, cols, *args)
    return plain(rows * cols, *args)


def solution(mesh):
    in_specs = (P(None, AXES, None), P(), P(), P(), P())
    body = functools.partial(local, mesh.shape["row"], mesh.shape["col"])
    return jax.shard_map(body, mesh=mesh, in_specs=in_specs, out_specs=P(None, AXES, None), check_vma=False)
```

time: 241 us -> 205 us (0.85)
  Pallas kernels: 32.5 us -> 195 us
  waiting for transfers between devices: 126 us -> 0 us
  matrix products: 46.5 us -> 0 us
  starting transfers between devices: 19.7 us -> 0 us
  other arithmetic: 11 us -> 0.67 us
  local copies, waits for them, and re-layouts: 4.42 us -> 8.44 us
    pallas_call x4 -> x1, Pallas kernels: 32.5 us -> 195 us  [fused(): pl.pallas_call(functools.partial(mixer_kernel, rows, cols), in_specs=[hbm...]
    all_to_all x4 -> x0, waiting for transfers between devices: 126 us -> none  [exchange(): return lax.all_to_all(x, AXES, split_axis=0, concat_axis=0, tiled=True)]
    dot_general x5 -> x0, matrix products: 46.5 us -> none  [the longest x1 26.3 us: local(): jnp.dot(norm(tokens), gate_weight, preferred_element_type=F32)]
    all_to_all x4 -> x0, starting transfers between devices: 19.7 us -> none  [exchange(): return lax.all_to_all(x, AXES, split_axis=0, concat_axis=0, tiled=True)]
    reduce_sum x2 -> x0, other arithmetic: 10.1 us -> none  [norm(): jnp.mean(widened * widened, axis=-1, keepdims=True) + 1e-06]
    unnamed x28 -> x1, local copies, waits for them, and re-layouts: 4.42 us -> 8.44 us
  transfers between devices with their start and end apart: 4 -> 0, of which waited for: 4 -> 0; matrix products, arithmetic and copies ran while one was open for 19% -> 0% of each run, Pallas kernels for 10% -> 0%
where the time goes in v1:
time: 205 us
  Pallas kernels  195 us (95%)
  local copies, waits for them, and re-layouts  8.44 us (4%)
    pallas_call x1, Pallas kernels, fused(): pl.pallas_call(functools.partial(mixer_kernel, rows, cols), in_specs=[hbm...  195 us
    unnamed x1, local copies, waits for them, and re-layouts  8.44 us

profile of v1, /device:TPU:0, one launch (start us, length us, event | category | flops | bytes accessed | tf_op | source)
XLA Modules:
  0.0 204.6 jit_solution(10242527877790597384)
XLA Ops:
  0.0 0.7 fusion.eye_in
  0.7 195.4 %mixer.1 = bf16[2,1024,2048]{2,1,0:T(8,128)(2,1)} custom-call(bf16[2,1024,2048]{2,1,0:T(8,128)(2,1)} %tokens.1, f32[1,2048]{1,0:T(1,128)} %bitcast.1, bf16[2048,1024]{1,0:T(8,128)(2,1)} %mix_in.1, bf16[2048,2048]{1,0:T(8,128)(2,1)} %gate_in.1, bf16[1024,2048]{1,0:T(8,128)(2,1)} %out_in.1, bf16[128,128]{1,0:T(8,128)(2,1)} %constant.12.clone.table_in, ...), custom_call_target="tpu_custom_call" | custom-call | tf_op jit(solution)/shard_map/mixer/pallas_call | solution.py:411
  196.1 8.4 %copy.13 = bf16[2,1024,2048]{2,1,0:T(8,128)(2,1)} copy(bf16[2,1024,2048]{2,1,0:T(8,128)(2,1)} %mixer.1) | data formatting | bytes 16777216

commit v2 on v1

--- a/solution.py
+++ b/solution.py
@@ -135,13 +135,12 @@
 def mixer_kernel(
     rows, cols, tokens, gain_in, mix_in, gate_in, out_in, table_in, order_in, eye_in, spread_in, cos_in, sin_in,
     close_in, result, token_v, normed, mix_v, gate_v, out_v, gain_v, table_v, order_v, eye_v, spread_v, cos_v, sin_v,
-    close_v, send_f, recv_f, send_r, recv_r, rows_in, rows_out, left_v, stage, load_sem, token_sem, stage_sem,
-    send_f_sem, recv_f_sem, send_r_sem, recv_r_sem,
+    close_v, send_f, recv_f, send_r, recv_r, rows_in, rows_out, left_v, load_sem, mix_sem, token_sem, send_f_sem, recv_f_sem, send_r_sem, recv_r_sem,
 ):
     devices = rows * cols
     row, col = lax.axis_index("row"), lax.axis_index("col")
     me = row * cols + col
-    parts, tile, width = stage.shape[0], token_v.shape[1], token_v.shape[2]
+    tile, width = token_v.shape[1], token_v.shape[2]
     tiles = send_f.shape[0]
     seqs = tokens.shape[0]
     per_seq = tiles // seqs
@@ -162,24 +161,43 @@
         pl.semaphore_signal(barrier, inc=1, device_id=(there_row, there_col), device_id_type=MESH)
         return carry
 
+    def positions(i):
+        return pl.ds(pl.multiple_of(lax.rem(i, per_seq) * tile, tile), tile)
+
     def token_load(i):
         slot = lax.rem(i, 2)
-        start = pl.multiple_of(lax.rem(i, per_seq) * tile, tile)
         return pltpu.make_async_copy(
-            tokens.at[i // per_seq, pl.ds(start, tile), :], token_v.at[slot], token_sem.at[slot]
+            tokens.at[i // per_seq, positions(i), :], token_v.at[slot], token_sem.at[slot]
         )
+
+    span = WIDE // channels
+    chunks = devices // span
+    mine, within = me // span, lax.rem(me, span)
+
+    def chunk_at(step):
+        shift = jnp.where(step == 0, chunks // 2, step + jnp.where(step >= chunks // 2, 1, 0))
+        return lax.rem(mine + shift, chunks)
+
+    def wide(n):
+        return pl.ds(pl.multiple_of(n * WIDE, WIDE), WIDE)
+
+    def mix_load(step):
+        these = wide(chunk_at(step))
+        return pltpu.make_async_copy(mix_in.at[:, these], mix_v.at[:, these], mix_sem.at[step])
 
     loads = [
         pltpu.make_async_copy(here, there, load_sem.at[at])
         for at, (here, there) in enumerate([
-            (gain_in, gain_v), (mix_in, mix_v), (table_in, table_v), (spread_in, spread_v), (cos_in, cos_v),
-            (sin_in, sin_v), (close_in, close_v), (gate_in, gate_v), (out_in, out_v), (order_in, order_v),
-            (eye_in, eye_v),
+            (gain_in, gain_v), (table_in, table_v), (spread_in, spread_v), (cos_in, cos_v), (sin_in, sin_v),
+            (close_in, close_v), (gate_in, gate_v), (out_in, out_v), (order_in, order_v), (eye_in, eye_v),
         ])
     ]
     token_load(0).start()
-    for load in loads[:3]:
-        load.start()
+    loads[0].start()
+    loads[1].start()
+    for step in range(chunks):
+        mix_load(step).start()
+    token_load(1).start()
     lax.fori_loop(1, devices, greet, 0)
 
     def norm(i):
@@ -190,64 +208,87 @@
             at = pl.ds(pl.multiple_of(r * 32, 32), 32)
             widened = token_v[slot, at, :].astype(F32)
             inverse_rms = lax.rsqrt(jnp.mean(widened * widened, axis=-1, keepdims=True) + 1e-06)
-            normed[i + 1, at, :] = (widened * inverse_rms * gain_v[...]).astype(BF16)
+            normed[i, at, :] = (widened * inverse_rms * gain_v[...]).astype(BF16)
             return carry
 
         lax.fori_loop(0, tile // 32, strip, 0)
 
+    def send_chunk(send_ref, recv_ref, send_sem, recv_sem, i, chunk):
+        def one(k, carry):
+            there = chunk * span + lax.rem(within + k, span)
+            there_row, there_col = there // cols, lax.rem(there, cols)
+
+            @pl.when(there != me)
+            def _():
+                pltpu.make_async_remote_copy(
+                    src_ref=send_ref.at[i, there], dst_ref=recv_ref.at[i, me], send_sem=send_sem.at[i],
+                    recv_sem=recv_sem.at[i], device_id=(there_row, there_col), device_id_type=MESH,
+                ).start()
+
+            return carry
+
+        lax.fori_loop(0, span, one, 0)
+
     def send(send_ref, recv_ref, send_sem, recv_sem, i):
-        def one(k, carry):
-            there_row, there_col, there = partner(k)
-            pltpu.make_async_remote_copy(
-                src_ref=send_ref.at[i, there], dst_ref=recv_ref.at[i, me], send_sem=send_sem.at[i],
-                recv_sem=recv_sem.at[i], device_id=(there_row, there_col), device_id_type=MESH,
-            ).start()
+        def one(step, carry):
+            send_chunk(send_ref, recv_ref, send_sem, recv_sem, i, chunk_at(step))
             return carry
 
         recv_ref[i, me] = send_ref[i, me]
-        lax.fori_loop(1, devices, one, 0)
+        lax.fori_loop(0, chunks, one, 0)
 
     def await_all(ref, sem, i):
         others = ref.at[i, pl.ds(0, devices - 1)]
         pltpu.make_async_copy(others, others, sem.at[i]).wait()
 
-    loads[0].wait()
-    norm(0)
-    token_load(1).start()
-    for load in loads[3:]:
-        load.start()
-    loads[1].wait()
-    loads[2].wait()
-    pl.semaphore_wait(barrier, devices - 1)
-
-    def forward(i, carry):
-        def columns(n, carry):
-            at = pl.ds(pl.multiple_of(n * WIDE, WIDE), WIDE)
-            mixed_in = jnp.dot(normed[i + 1], mix_v[:, at], preferred_element_type=F32).astype(BF16)
-            for part in range(WIDE // GROUP_DIM):
-                turned = lax.dot_general(
-                    table_v[...], mixed_in[:, part * GROUP_DIM : (part + 1) * GROUP_DIM], NT,
-                    preferred_element_type=F32,
-                ).astype(BF16)
-                owner = (n * (WIDE // GROUP_DIM) + part) * per_group
-                send_f[i, pl.ds(owner, per_group)] = turned.reshape(per_group, channels, tile)
-            return carry
-
-        lax.fori_loop(0, mixed // WIDE, columns, 0)
-        send(send_f, recv_f, send_f_sem, recv_f_sem, i)
-
-        @pl.when(i + 1 < tiles)
+    def compute(m):
+        i, step = m // chunks, lax.rem(m, chunks)
+
+        @pl.when(step == 0)
         def _():
+            norm(i)
+
             @pl.when(i + 2 < tiles)
             def _():
                 token_load(i + 2).start()
 
-            norm(i + 1)
+        @pl.when(i == 0)
+        def _():
+            mix_load(step).wait()
+
+        n = chunk_at(step)
+        mixed_in = jnp.dot(normed[i], mix_v[:, wide(n)], preferred_element_type=F32).astype(BF16)
+        for part in range(WIDE // GROUP_DIM):
+            turned = lax.dot_general(
+                table_v[...], mixed_in[:, part * GROUP_DIM : (part + 1) * GROUP_DIM], NT,
+                preferred_element_type=F32,
+            ).astype(BF16)
+            send_f[i, pl.ds(n * span + part * per_group, per_group)] = turned.reshape(per_group, channels, tile)
+
+    def forward(m, carry):
+        i, step = m // chunks, lax.rem(m, chunks)
+        n = chunk_at(step)
+
+        @pl.when(n == mine)
+        def _():
+            recv_f[i, me] = send_f[i, me]
+
+        send_chunk(send_f, recv_f, send_f_sem, recv_f_sem, i, n)
+
+        @pl.when(m + 1 < tiles * chunks)
+        def _():
+            compute(m + 1)
 
         return carry
 
-    lax.fori_loop(0, tiles, forward, 0)
-    for load in loads[3:]:
+    loads[0].wait()
+    loads[1].wait()
+    compute(0)
+    for load in loads[2:]:
+        load.start()
+    pl.semaphore_wait(barrier, devices - 1)
+    lax.fori_loop(0, tiles * chunks, forward, 0)
+    for load in loads[2:]:
         load.wait()
 
     for group in range(mixed // GROUP_DIM):
@@ -317,9 +358,9 @@
 
         def gate(at, carry):
             i, n = seq * per_seq + at // (width // WIDE), lax.rem(at, width // WIDE)
-            these = pl.ds(pl.multiple_of(n * WIDE, WIDE), WIDE)
-            logits = jnp.dot(normed[i + 1], gate_v[:, these], preferred_element_type=F32)
-            normed[i, :, these] = jax.nn.sigmoid(logits).astype(BF16)
+            these = wide(n)
+            logits = jnp.dot(normed[i], gate_v[:, these], preferred_element_type=F32)
+            result[seq, positions(i), these] = jax.nn.sigmoid(logits).astype(BF16)
             return carry
 
         lax.fori_loop(0, per_seq * (width // WIDE), gate, 0)
@@ -327,37 +368,22 @@
 
     lax.fori_loop(0, seqs, middle, 0)
 
-    def put(j):
-        slot = lax.rem(j, parts)
-        start = pl.multiple_of(lax.rem(j, per_seq) * tile, tile)
-        return pltpu.make_async_copy(
-            stage.at[slot], result.at[j // per_seq, pl.ds(start, tile), :], stage_sem.at[slot]
-        )
-
     def finish(j, carry):
-        slot = lax.rem(j, parts)
         await_all(recv_r, recv_r_sem, j)
-
-        @pl.when(j >= parts)
-        def _():
-            put(j - parts).wait()
-
         left = jnp.concatenate([recv_r[j, :, low].reshape(mixed, LANES) for low in range(lows)], axis=1)
         left_v[...] = lax.dot_general(eye_v[...], left, NT, preferred_element_type=F32).astype(BF16)
 
         def columns(n, carry):
-            these = pl.ds(pl.multiple_of(n * WIDE, WIDE), WIDE)
+            these = wide(n)
             mapped = jnp.dot(left_v[...], out_v[:, these], preferred_element_type=F32)
-            stage[slot, :, these] = (normed[j, :, these].astype(F32) * mapped).astype(BF16)
+            at = (j // per_seq, positions(j), these)
+            result[at] = (result[at].astype(F32) * mapped).astype(BF16)
             return carry
 
         lax.fori_loop(0, width // WIDE, columns, 0)
-        put(j).start()
         return carry
 
     lax.fori_loop(0, tiles, finish, 0)
-    for j in range(tiles - parts, tiles):
-        put(j).wait()
     for i in range(tiles):
         await_all(send_f, send_f_sem, i)
         await_all(send_r, send_r_sem, i)
@@ -378,7 +404,7 @@
     constants = [
         jnp.asarray(channel_table().T, BF16),
         jnp.asarray(channel_order(), BF16),
-        jnp.eye(tile, dtype=BF16),
+        jnp.asarray(np.eye(tile), BF16),
         jnp.asarray(np.stack([lone.T, normal.T]), BF16),
         jnp.asarray(cosine.T, F32),
         jnp.asarray(sine.T, F32),
@@ -386,10 +412,9 @@
     ]
     operands = [tokens, norm_gain.reshape(1, width), mix_weight, gate_weight, out_weight, *constants]
     hbm = pl.BlockSpec(memory_space=pl.ANY)
-    parts = 2
     scratch = [
         pltpu.VMEM((2, tile, width), BF16),
-        pltpu.VMEM((tiles + 1, tile, width), BF16),
+        pltpu.VMEM((tiles, tile, width), BF16),
         pltpu.VMEM(mix_weight.shape, BF16),
         pltpu.VMEM(gate_weight.shape, BF16),
         pltpu.VMEM(out_weight.shape, BF16),
@@ -402,20 +427,19 @@
         pltpu.VMEM((here // LANES, devices * BLOCK, LANES), F32),
         pltpu.VMEM((second * BLOCK, first), F32),
         pltpu.VMEM((tile, mixed), BF16),
-        pltpu.VMEM((parts, tile, width), BF16),
-        pltpu.SemaphoreType.DMA((4 + len(constants),)),
+        pltpu.SemaphoreType.DMA((3 + len(constants),)),
+        pltpu.SemaphoreType.DMA((mixed // WIDE,)),
         pltpu.SemaphoreType.DMA((2,)),
-        pltpu.SemaphoreType.DMA((parts,)),
         *[pltpu.SemaphoreType.DMA((tiles,)) for _ in range(4)],
     ]
     return pl.pallas_call(
         functools.partial(mixer_kernel, rows, cols),
         in_specs=[hbm] * len(operands),
-        out_specs=hbm,
-        out_shape=jax.ShapeDtypeStruct(tokens.shape, BF16),
+        out_specs=pl.BlockSpec(memory_space=pltpu.VMEM),
+        out_shape=pltpu.VMEM(tokens.shape, BF16),
         scratch_shapes=scratch,
         compiler_params=pltpu.CompilerParams(
-            collective_id=0, has_side_effects=True, vmem_limit_bytes=60 * 2**20
+            collective_id=0, has_side_effects=True, vmem_limit_bytes=54 * 2**20
         ),
         name="mixer",
     )(*operands)

time: 205 us -> 194 us (0.946)
  local copies, waits for them, and re-layouts: 8.44 us -> 3.4 us
  Pallas kernels: 195 us -> 190 us
    unnamed x1, local copies, waits for them, and re-layouts: 8.44 us -> 3.4 us
    pallas_call x1, Pallas kernels: 195 us -> 190 us  [fused(): pl.pallas_call(functools.partial(mixer_kernel, rows, cols), in_specs=[hbm...]
where the time goes in v2:
time: 194 us
  Pallas kernels  190 us (98%)
  local copies, waits for them, and re-layouts  3.4 us (2%)
    pallas_call x1, Pallas kernels, fused(): pl.pallas_call(functools.partial(mixer_kernel, rows, cols), in_specs=[hbm...  190 us

profile of v2, /device:TPU:0, one launch (start us, length us, event | category | flops | bytes accessed | tf_op | source)
XLA Modules:
  0.0 193.8 jit_solution(3117280658706936841)
XLA Ops:
  0.0 190.4 %mixer.1 = bf16[2,1024,2048]{2,1,0:T(8,128)(2,1)S(1)} custom-call(bf16[2,1024,2048]{2,1,0:T(8,128)(2,1)} %tokens.1, f32[1,2048]{1,0:T(1,128)} %bitcast.1, bf16[2048,1024]{1,0:T(8,128)(2,1)} %mix_in.1, bf16[2048,2048]{1,0:T(8,128)(2,1)} %gate_in.1, bf16[1024,2048]{1,0:T(8,128)(2,1)} %out_in.1, bf16[128,128]{1,0:T(8,128)(2,1)} %constant.14.clone.table_in, ...), custom_call_target="tpu_custom_call" | custom-call | tf_op jit(solution)/shard_map/mixer/pallas_call | solution.py:435
  190.4 3.4 %copy.14 = bf16[2,1024,2048]{2,1,0:T(8,128)(2,1)} copy(bf16[2,1024,2048]{2,1,0:T(8,128)(2,1)S(1)} %mixer.1) | data formatting | bytes 16777216

commit v3 on v2

--- a/solution.py
+++ b/solution.py
@@ -134,8 +134,8 @@
 
 def mixer_kernel(
     rows, cols, tokens, gain_in, mix_in, gate_in, out_in, table_in, order_in, eye_in, spread_in, cos_in, sin_in,
-    close_in, result, token_v, normed, mix_v, gate_v, out_v, gain_v, table_v, order_v, eye_v, spread_v, cos_v, sin_v,
-    close_v, send_f, recv_f, send_r, recv_r, rows_in, rows_out, left_v, load_sem, mix_sem, token_sem, send_f_sem, recv_f_sem, send_r_sem, recv_r_sem,
+    close_in, result, left_v, out_v, token_v, normed, mix_v, gate_v, gain_v, table_v, order_v, eye_v, spread_v, cos_v,
+    sin_v, close_v, send_f, recv_f, send_r, recv_r, rows_in, rows_out, load_sem, mix_sem, token_sem, send_f_sem, recv_f_sem, send_r_sem, recv_r_sem,
 ):
     devices = rows * cols
     row, col = lax.axis_index("row"), lax.axis_index("col")
@@ -152,14 +152,22 @@
 
     barrier = pltpu.get_barrier_semaphore()
 
-    def partner(k):
-        there_row, there_col = lax.rem(row + lax.rem(k, rows), rows), lax.rem(col + k // rows, cols)
-        return there_row, there_col, there_row * cols + there_col
-
-    def greet(k, carry):
-        there_row, there_col, _ = partner(k)
-        pl.semaphore_signal(barrier, inc=1, device_id=(there_row, there_col), device_id_type=MESH)
-        return carry
+    span = WIDE // channels
+    chunks = devices // span
+    mine, within = me // span, lax.rem(me, span)
+
+    def partner(chunk, k):
+        there = chunk * span + lax.rem(within + k, span)
+        return there, (there // cols, lax.rem(there, cols))
+
+    for shift in range(chunks):
+        far = lax.rem(2 * chunks - 1 - mine + shift, chunks)
+        for k in range(span):
+            there, address = partner(far, k)
+
+            @pl.when(there != me)
+            def _():
+                pl.semaphore_signal(barrier, inc=1, device_id=address, device_id_type=MESH)
 
     def positions(i):
         return pl.ds(pl.multiple_of(lax.rem(i, per_seq) * tile, tile), tile)
@@ -169,10 +177,6 @@
         return pltpu.make_async_copy(
             tokens.at[i // per_seq, positions(i), :], token_v.at[slot], token_sem.at[slot]
         )
-
-    span = WIDE // channels
-    chunks = devices // span
-    mine, within = me // span, lax.rem(me, span)
 
     def chunk_at(step):
         shift = jnp.where(step == 0, chunks // 2, step + jnp.where(step >= chunks // 2, 1, 0))
@@ -198,7 +202,6 @@
     for step in range(chunks):
         mix_load(step).start()
     token_load(1).start()
-    lax.fori_loop(1, devices, greet, 0)
 
     def norm(i):
         slot = lax.rem(i, 2)
@@ -215,14 +218,13 @@
 
     def send_chunk(send_ref, recv_ref, send_sem, recv_sem, i, chunk):
         def one(k, carry):
-            there = chunk * span + lax.rem(within + k, span)
-            there_row, there_col = there // cols, lax.rem(there, cols)
+            there, address = partner(chunk, k)
 
             @pl.when(there != me)
             def _():
                 pltpu.make_async_remote_copy(
                     src_ref=send_ref.at[i, there], dst_ref=recv_ref.at[i, me], send_sem=send_sem.at[i],
-                    recv_sem=recv_sem.at[i], device_id=(there_row, there_col), device_id_type=MESH,
+                    recv_sem=recv_sem.at[i], device_id=address, device_id_type=MESH,
                 ).start()
 
             return carry
@@ -265,9 +267,8 @@
             ).astype(BF16)
             send_f[i, pl.ds(n * span + part * per_group, per_group)] = turned.reshape(per_group, channels, tile)
 
-    def forward(m, carry):
-        i, step = m // chunks, lax.rem(m, chunks)
-        n = chunk_at(step)
+    def post(m):
+        i, n = m // chunks, chunk_at(lax.rem(m, chunks))
 
         @pl.when(n == mine)
         def _():
@@ -275,21 +276,27 @@
 
         send_chunk(send_f, recv_f, send_f_sem, recv_f_sem, i, n)
 
-        @pl.when(m + 1 < tiles * chunks)
+    def forward(m, carry):
+        compute(m + 1)
+
+        @pl.when(m > 0)
         def _():
-            compute(m + 1)
+            post(m)
 
         return carry
 
+    pieces = tiles * chunks
     loads[0].wait()
     loads[1].wait()
     compute(0)
     for load in loads[2:]:
         load.start()
     pl.semaphore_wait(barrier, devices - 1)
-    lax.fori_loop(0, tiles * chunks, forward, 0)
+    post(0)
+    lax.fori_loop(0, pieces - 1, forward, 0)
     for load in loads[2:]:
         load.wait()
+    post(pieces - 1)
 
     for group in range(mixed // GROUP_DIM):
         at = pl.ds(group * GROUP_DIM, GROUP_DIM)
@@ -353,9 +360,6 @@
         for t in range(per_seq):
             await_all(recv_f, recv_f_sem, seq * per_seq + t)
         transform(seq)
-        for q in range(per_seq):
-            send(send_r, recv_r, send_r_sem, recv_r_sem, seq * per_seq + q)
-
         def gate(at, carry):
             i, n = seq * per_seq + at // (width // WIDE), lax.rem(at, width // WIDE)
             these = wide(n)
@@ -364,29 +368,59 @@
             return carry
 
         lax.fori_loop(0, per_seq * (width // WIDE), gate, 0)
+        for q in range(per_seq):
+            send(send_r, recv_r, send_r_sem, recv_r_sem, seq * per_seq + q)
         return carry
 
     lax.fori_loop(0, seqs, middle, 0)
 
-    def finish(j, carry):
+    def gather(j):
         await_all(recv_r, recv_r_sem, j)
         left = jnp.concatenate([recv_r[j, :, low].reshape(mixed, LANES) for low in range(lows)], axis=1)
         left_v[...] = lax.dot_general(eye_v[...], left, NT, preferred_element_type=F32).astype(BF16)
 
+    def finish(j, carry):
+        gather(j)
+
         def columns(n, carry):
-            these = wide(n)
-            mapped = jnp.dot(left_v[...], out_v[:, these], preferred_element_type=F32)
-            at = (j // per_seq, positions(j), these)
+            at = (j // per_seq, positions(j), wide(n))
+            mapped = jnp.dot(left_v[...], out_v[:, wide(n)], preferred_element_type=F32)
             result[at] = (result[at].astype(F32) * mapped).astype(BF16)
             return carry
 
         lax.fori_loop(0, width // WIDE, columns, 0)
         return carry
 
-    lax.fori_loop(0, tiles, finish, 0)
+    lax.fori_loop(0, tiles - 1, finish, 0)
+    gather(tiles - 1)
     for i in range(tiles):
         await_all(send_f, send_f_sem, i)
         await_all(send_r, send_r_sem, i)
+
+
+def last_kernel(gated, left, out_v, final, stage, sems):
+    tile, width = stage.shape
+    per_seq = gated.shape[1] // tile
+    tiles = sems.shape[0]
+
+    def put(j):
+        at = (j // per_seq, pl.ds(j % per_seq * tile, tile))
+        return pltpu.make_async_copy(gated.at[at] if j + 1 < tiles else stage, final.at[at], sems.at[j])
+
+    for j in range(tiles - 1):
+        put(j).start()
+
+    def columns(n, carry):
+        at = pl.ds(pl.multiple_of(n * WIDE, WIDE), WIDE)
+        mapped = jnp.dot(left[...], out_v[:, at], preferred_element_type=F32)
+        gate = gated[gated.shape[0] - 1, gated.shape[1] - tile :, at].astype(F32)
+        stage[:, at] = (gate * mapped).astype(BF16)
+        return carry
+
+    lax.fori_loop(0, width // WIDE, columns, 0)
+    put(tiles - 1).start()
+    for j in range(tiles):
+        put(j).wait()
 
 
 def fused(rows, cols, tokens, norm_gain, mix_weight, gate_weight, out_weight):
@@ -417,7 +451,6 @@
         pltpu.VMEM((tiles, tile, width), BF16),
         pltpu.VMEM(mix_weight.shape, BF16),
         pltpu.VMEM(gate_weight.shape, BF16),
-        pltpu.VMEM(out_weight.shape, BF16),
         pltpu.VMEM((1, width), F32),
         *[pltpu.VMEM(constant.shape, constant.dtype) for constant in constants],
         pltpu.VMEM((tiles, devices, channels, tile), BF16),
@@ -426,23 +459,34 @@
         pltpu.VMEM((tiles, devices, lows, channels, first), BF16),
         pltpu.VMEM((here // LANES, devices * BLOCK, LANES), F32),
         pltpu.VMEM((second * BLOCK, first), F32),
-        pltpu.VMEM((tile, mixed), BF16),
         pltpu.SemaphoreType.DMA((3 + len(constants),)),
         pltpu.SemaphoreType.DMA((mixed // WIDE,)),
         pltpu.SemaphoreType.DMA((2,)),
         *[pltpu.SemaphoreType.DMA((tiles,)) for _ in range(4)],
     ]
-    return pl.pallas_call(
+    vmem = pl.BlockSpec(memory_space=pltpu.VMEM)
+    made = pl.pallas_call(
         functools.partial(mixer_kernel, rows, cols),
         in_specs=[hbm] * len(operands),
-        out_specs=pl.BlockSpec(memory_space=pltpu.VMEM),
-        out_shape=pltpu.VMEM(tokens.shape, BF16),
+        out_specs=[vmem] * 3,
+        out_shape=[
+            pltpu.VMEM(tokens.shape, BF16), pltpu.VMEM((tile, mixed), BF16), pltpu.VMEM(out_weight.shape, BF16)
+        ],
         scratch_shapes=scratch,
         compiler_params=pltpu.CompilerParams(
-            collective_id=0, has_side_effects=True, vmem_limit_bytes=54 * 2**20
+            collective_id=0, has_side_effects=True, vmem_limit_bytes=48 * 2**20
         ),
         name="mixer",
     )(*operands)
+    return pl.pallas_call(
+        last_kernel,
+        in_specs=[vmem] * 3,
+        out_specs=hbm,
+        out_shape=jax.ShapeDtypeStruct(tokens.shape, BF16),
+        scratch_shapes=[pltpu.VMEM((tile, width), BF16), pltpu.SemaphoreType.DMA((tiles,))],
+        compiler_params=pltpu.CompilerParams(vmem_limit_bytes=4 * 2**20),
+        name="last",
+    )(*[pltpu.with_memory_space_constraint(array, pltpu.VMEM) for array in made])
 
 
 def fits(devices, tokens, mix_weight):

time: 194 us -> 192 us (0.990)
  local copies, waits for them, and re-layouts: 3.4 us -> 0 us
  Pallas kernels: 190 us -> 192 us
    pallas_call x0 -> x1, Pallas kernels: none -> 3.59 us  [fused(): pl.pallas_call(last_kernel, in_specs=[vmem] * 3, out_specs=hbm, out_shape...]
    unnamed x1 -> x0, local copies, waits for them, and re-layouts: 3.4 us -> none
    pallas_call x1, Pallas kernels: 190 us -> 188 us  [fused(): pl.pallas_call(functools.partial(mixer_kernel, rows, cols), in_specs=[hbm...]
where the time goes in v3:
time: 192 us
  Pallas kernels  192 us (100%)
    pallas_call x1, Pallas kernels, fused(): pl.pallas_call(functools.partial(mixer_kernel, rows, cols), in_specs=[hbm...  188 us

profile of v3, /device:TPU:0, one launch (start us, length us, event | category | flops | bytes accessed | tf_op | source)
XLA Modules:
  0.0 191.9 jit_solution(3005411461194267654)
XLA Ops:
  0.0 188.3 %mixer.1 = (bf16[2,1024,2048]{2,1,0:T(8,128)(2,1)S(1)}, bf16[256,1024]{1,0:T(8,128)(2,1)S(1)}, bf16[1024,2048]{1,0:T(8,128)(2,1)S(1)}) custom-call(bf16[2,1024,2048]{2,1,0:T(8,128)(2,1)} %tokens.1, f32[1,2048]{1,0:T(1,128)} %bitcast.1, bf16[2048,1024]{1,0:T(8,128)(2,1)} %mix_in.1, bf16[2048,2048]{1,0:T(8,128)(2,1)} %gate_in.1, bf16[1024,2048]{1,0:T(8,128)(2,1)} %out_in.1, ...), custom_call_target="tpu_custom_call" | custom-call | tf_op jit(solution)/shard_map/mixer/pallas_call | solution.py:468
  188.3 3.6 %last.1 = bf16[2,1024,2048]{2,1,0:T(8,128)(2,1)} custom-call(bf16[2,1024,2048]{2,1,0:T(8,128)(2,1)S(1)} %get-tuple-element.8.gated, bf16[256,1024]{1,0:T(8,128)(2,1)S(1)} %get-tuple-element.9.left, bf16[1024,2048]{1,0:T(8,128)(2,1)S(1)} %get-tuple-element.10.out_v), custom_call_target="tpu_custom_call" | custom-call | tf_op jit(solution)/shard_map/last/pallas_call | solution.py:481

commit v4 on v3

--- a/solution.py
+++ b/solution.py
@@ -135,7 +135,7 @@
 def mixer_kernel(
     rows, cols, tokens, gain_in, mix_in, gate_in, out_in, table_in, order_in, eye_in, spread_in, cos_in, sin_in,
     close_in, result, left_v, out_v, token_v, normed, mix_v, gate_v, gain_v, table_v, order_v, eye_v, spread_v, cos_v,
-    sin_v, close_v, send_f, recv_f, send_r, recv_r, rows_in, rows_out, load_sem, mix_sem, token_sem, send_f_sem, recv_f_sem, send_r_sem, recv_r_sem,
+    sin_v, close_v, send_f, recv_f, send_r, recv_r, rows_in, rows_out, load_sem, mix_sem, token_sem, send_f_sem, recv_f_sem, send_r_sem, recv_r_sem, word,
 ):
     devices = rows * cols
     row, col = lax.axis_index("row"), lax.axis_index("col")
@@ -160,14 +160,26 @@
         there = chunk * span + lax.rem(within + k, span)
         return there, (there // cols, lax.rem(there, cols))
 
-    for shift in range(chunks):
-        far = lax.rem(2 * chunks - 1 - mine + shift, chunks)
+    last = chunks - 1
+    relay = (last - 1) * span + 1
+    relay_address = (relay // cols, relay % cols)
+
+    def tell(chunk, semaphore):
         for k in range(span):
-            there, address = partner(far, k)
+            there, address = partner(chunk, k)
 
             @pl.when(there != me)
             def _():
-                pl.semaphore_signal(barrier, inc=1, device_id=address, device_id_type=MESH)
+                pl.semaphore_signal(semaphore, inc=1, device_id=address, device_id_type=MESH)
+
+    @pl.when(mine != last)
+    def _():
+        for shift in range(last):
+            tell(lax.rem(2 * last - 1 - mine + shift, last), barrier)
+
+    @pl.when(mine == last)
+    def _():
+        pl.semaphore_signal(barrier, inc=1, device_id=relay_address, device_id_type=MESH)
 
     def positions(i):
         return pl.ds(pl.multiple_of(lax.rem(i, per_seq) * tile, tile), tile)
@@ -178,9 +190,20 @@
             tokens.at[i // per_seq, positions(i), :], token_v.at[slot], token_sem.at[slot]
         )
 
+    half = chunks // 2
+
+    def shifted(step):
+        return lax.rem(mine + jnp.where(step == 0, half, step + jnp.where(step >= half, 1, 0)), chunks)
+
+    away = last - mine
+    turn = jnp.where(away == half, 0, jnp.where(away == 0, last, jnp.where(away > half, away - 1, away)))
+
     def chunk_at(step):
-        shift = jnp.where(step == 0, chunks // 2, step + jnp.where(step >= chunks // 2, 1, 0))
-        return lax.rem(mine + shift, chunks)
+        return jnp.where(step == last, last, shifted(step + jnp.where(step >= turn, 1, 0)))
+
+    def chunk_back(step):
+        passing = step + 1 + jnp.where(step + 1 >= half, 1, 0)
+        return lax.rem(mine + jnp.where(step == last, 0, jnp.where(step == last - 1, half, passing)), chunks)
 
     def wide(n):
         return pl.ds(pl.multiple_of(n * WIDE, WIDE), WIDE)
@@ -233,7 +256,7 @@
 
     def send(send_ref, recv_ref, send_sem, recv_sem, i):
         def one(step, carry):
-            send_chunk(send_ref, recv_ref, send_sem, recv_sem, i, chunk_at(step))
+            send_chunk(send_ref, recv_ref, send_sem, recv_sem, i, chunk_back(step))
             return carry
 
         recv_ref[i, me] = send_ref[i, me]
@@ -274,6 +297,10 @@
         def _():
             recv_f[i, me] = send_f[i, me]
 
+        @pl.when(jnp.logical_and(m == last, jnp.logical_and(mine != last, me != relay)))
+        def _():
+            pl.semaphore_wait(word, 1)
+
         send_chunk(send_f, recv_f, send_f_sem, recv_f_sem, i, n)
 
     def forward(m, carry):
@@ -291,7 +318,22 @@
     compute(0)
     for load in loads[2:]:
         load.start()
-    pl.semaphore_wait(barrier, devices - 1)
+
+    @pl.when(me == relay)
+    def _():
+        pl.semaphore_wait(barrier, devices - 1)
+        tell(last, barrier)
+        for chunk in range(last):
+            tell(chunk, word)
+
+    @pl.when(jnp.logical_and(mine != last, me != relay))
+    def _():
+        pl.semaphore_wait(barrier, devices - span - 1)
+
+    @pl.when(mine == last)
+    def _():
+        pl.semaphore_wait(barrier, 1)
+
     post(0)
     lax.fori_loop(0, pieces - 1, forward, 0)
     for load in loads[2:]:
@@ -463,6 +505,7 @@
         pltpu.SemaphoreType.DMA((mixed // WIDE,)),
         pltpu.SemaphoreType.DMA((2,)),
         *[pltpu.SemaphoreType.DMA((tiles,)) for _ in range(4)],
+        pltpu.SemaphoreType.REGULAR,
     ]
     vmem = pl.BlockSpec(memory_space=pltpu.VMEM)
     made = pl.pallas_call(
@@ -501,6 +544,7 @@
         and here % second == 0
         and here // second == GROUP_DIM // devices
         and mixed % WIDE == 0
+        and mixed // WIDE >= 4
         and width % WIDE == 0
     )
 

time: 192 us -> 194 us (1.010)
  Pallas kernels: 192 us -> 194 us
    pallas_call x1, Pallas kernels: 188 us -> 191 us  [fused(): pl.pallas_call(functools.partial(mixer_kernel, rows, cols), in_specs=[hbm...]
where the time goes in v4:
time: 194 us
  Pallas kernels  194 us (100%)
    pallas_call x1, Pallas kernels, fused(): pl.pallas_call(functools.partial(mixer_kernel, rows, cols), in_specs=[hbm...  191 us

profile of v4, /device:TPU:0, one launch (start us, length us, event | category | flops | bytes accessed | tf_op | source)
XLA Modules:
  0.0 194.1 jit_solution(6068029527612404338)
XLA Ops:
  0.0 190.5 %mixer.1 = (bf16[2,1024,2048]{2,1,0:T(8,128)(2,1)S(1)}, bf16[256,1024]{1,0:T(8,128)(2,1)S(1)}, bf16[1024,2048]{1,0:T(8,128)(2,1)S(1)}) custom-call(bf16[2,1024,2048]{2,1,0:T(8,128)(2,1)} %tokens.1, f32[1,2048]{1,0:T(1,128)} %bitcast.1, bf16[2048,1024]{1,0:T(8,128)(2,1)} %mix_in.1, bf16[2048,2048]{1,0:T(8,128)(2,1)} %gate_in.1, bf16[1024,2048]{1,0:T(8,128)(2,1)} %out_in.1, ...), custom_call_target="tpu_custom_call" | custom-call | tf_op jit(solution)/shard_map/mixer/pallas_call | solution.py:511
  190.5 3.6 %last.1 = bf16[2,1024,2048]{2,1,0:T(8,128)(2,1)} custom-call(bf16[2,1024,2048]{2,1,0:T(8,128)(2,1)S(1)} %get-tuple-element.8.gated, bf16[256,1024]{1,0:T(8,128)(2,1)S(1)} %get-tuple-element.9.left, bf16[1024,2048]{1,0:T(8,128)(2,1)S(1)} %get-tuple-element.10.out_v), custom_call_target="tpu_custom_call" | custom-call | tf_op jit(solution)/shard_map/last/pallas_call | solution.py:524

commit v5 on v4

--- a/solution.py
+++ b/solution.py
@@ -172,15 +172,6 @@
             def _():
                 pl.semaphore_signal(semaphore, inc=1, device_id=address, device_id_type=MESH)
 
-    @pl.when(mine != last)
-    def _():
-        for shift in range(last):
-            tell(lax.rem(2 * last - 1 - mine + shift, last), barrier)
-
-    @pl.when(mine == last)
-    def _():
-        pl.semaphore_signal(barrier, inc=1, device_id=relay_address, device_id_type=MESH)
-
     def positions(i):
         return pl.ds(pl.multiple_of(lax.rem(i, per_seq) * tile, tile), tile)
 
@@ -198,18 +189,21 @@
     away = last - mine
     turn = jnp.where(away == half, 0, jnp.where(away == 0, last, jnp.where(away > half, away - 1, away)))
 
-    def chunk_at(step):
+    def chunk_first(step):
         return jnp.where(step == last, last, shifted(step + jnp.where(step >= turn, 1, 0)))
+
+    def chunk_at(i, step):
+        return jnp.where(i == 0, chunk_first(step), shifted(step))
 
     def chunk_back(step):
         passing = step + 1 + jnp.where(step + 1 >= half, 1, 0)
-        return lax.rem(mine + jnp.where(step == last, 0, jnp.where(step == last - 1, half, passing)), chunks)
+        return shifted(step)
 
     def wide(n):
         return pl.ds(pl.multiple_of(n * WIDE, WIDE), WIDE)
 
     def mix_load(step):
-        these = wide(chunk_at(step))
+        these = wide(chunk_first(step))
         return pltpu.make_async_copy(mix_in.at[:, these], mix_v.at[:, these], mix_sem.at[step])
 
     loads = [
@@ -222,7 +216,18 @@
     token_load(0).start()
     loads[0].start()
     loads[1].start()
-    for step in range(chunks):
+    mix_load(0).start()
+
+    @pl.when(mine != last)
+    def _():
+        for shift in range(last):
+            tell(lax.rem(2 * last - 1 - mine + shift, last), barrier)
+
+    @pl.when(mine == last)
+    def _():
+        pl.semaphore_signal(barrier, inc=1, device_id=relay_address, device_id_type=MESH)
+
+    for step in range(1, chunks):
         mix_load(step).start()
     token_load(1).start()
 
@@ -237,7 +242,7 @@
             normed[i, at, :] = (widened * inverse_rms * gain_v[...]).astype(BF16)
             return carry
 
-        lax.fori_loop(0, tile // 32, strip, 0)
+        lax.fori_loop(0, tile // 32, strip, 0, unroll=4)
 
     def send_chunk(send_ref, recv_ref, send_sem, recv_sem, i, chunk):
         def one(k, carry):
@@ -281,7 +286,7 @@
         def _():
             mix_load(step).wait()
 
-        n = chunk_at(step)
+        n = chunk_at(i, step)
         mixed_in = jnp.dot(normed[i], mix_v[:, wide(n)], preferred_element_type=F32).astype(BF16)
         for part in range(WIDE // GROUP_DIM):
             turned = lax.dot_general(
@@ -291,7 +296,7 @@
             send_f[i, pl.ds(n * span + part * per_group, per_group)] = turned.reshape(per_group, channels, tile)
 
     def post(m):
-        i, n = m // chunks, chunk_at(lax.rem(m, chunks))
+        i, n = m // chunks, chunk_at(m // chunks, lax.rem(m, chunks))
 
         @pl.when(n == mine)
         def _():

time: 194 us -> 191 us (0.985)
  Pallas kernels: 194 us -> 190 us
    pallas_call x1, Pallas kernels: 191 us -> 187 us  [fused(): pl.pallas_call(functools.partial(mixer_kernel, rows, cols), in_specs=[hbm...]
where the time goes in v5:
time: 191 us; the launch traced here: 190 us
  Pallas kernels  190 us (99%)
    pallas_call x1, Pallas kernels, fused(): pl.pallas_call(functools.partial(mixer_kernel, rows, cols), in_specs=[hbm...  187 us

profile of v5, /device:TPU:0, one launch (start us, length us, event | category | flops | bytes accessed | tf_op | source)
XLA Modules:
  0.0 190.4 jit_solution(16094508653062185319)
XLA Ops:
  0.0 186.7 %mixer.1 = (bf16[2,1024,2048]{2,1,0:T(8,128)(2,1)S(1)}, bf16[256,1024]{1,0:T(8,128)(2,1)S(1)}, bf16[1024,2048]{1,0:T(8,128)(2,1)S(1)}) custom-call(bf16[2,1024,2048]{2,1,0:T(8,128)(2,1)} %tokens.1, f32[1,2048]{1,0:T(1,128)} %bitcast.1, bf16[2048,1024]{1,0:T(8,128)(2,1)} %mix_in.1, bf16[2048,2048]{1,0:T(8,128)(2,1)} %gate_in.1, bf16[1024,2048]{1,0:T(8,128)(2,1)} %out_in.1, ...), custom_call_target="tpu_custom_call" | custom-call | tf_op jit(solution)/shard_map/mixer/pallas_call | solution.py:516
  186.8 3.6 %last.1 = bf16[2,1024,2048]{2,1,0:T(8,128)(2,1)} custom-call(bf16[2,1024,2048]{2,1,0:T(8,128)(2,1)S(1)} %get-tuple-element.8.gated, bf16[256,1024]{1,0:T(8,128)(2,1)S(1)} %get-tuple-element.9.left, bf16[1024,2048]{1,0:T(8,128)(2,1)S(1)} %get-tuple-element.10.out_v), custom_call_target="tpu_custom_call" | custom-call | tf_op jit(solution)/shard_map/last/pallas_call | solution.py:529

commit v6 on v5

--- a/solution.py
+++ b/solution.py
@@ -161,7 +161,7 @@
         return there, (there // cols, lax.rem(there, cols))
 
     last = chunks - 1
-    relay = (last - 1) * span + 1
+    relay = last * span - 1
     relay_address = (relay // cols, relay % cols)
 
     def tell(chunk, semaphore):
@@ -201,6 +201,12 @@
 
     def wide(n):
         return pl.ds(pl.multiple_of(n * WIDE, WIDE), WIDE)
+
+    fore = tile // 2
+
+    def token_half(part):
+        rows_at = pl.ds(part * fore, fore)
+        return pltpu.make_async_copy(tokens.at[0, rows_at, :], token_v.at[0, rows_at, :], token_sem.at[2 * part])
 
     def mix_load(step):
         these = wide(chunk_first(step))
@@ -213,10 +219,11 @@
             (close_in, close_v), (gate_in, gate_v), (out_in, out_v), (order_in, order_v), (eye_in, eye_v),
         ])
     ]
-    token_load(0).start()
+    token_half(0).start()
     loads[0].start()
     loads[1].start()
     mix_load(0).start()
+    token_half(1).start()
 
     @pl.when(mine != last)
     def _():
@@ -231,18 +238,23 @@
         mix_load(step).start()
     token_load(1).start()
 
-    def norm(i):
+    def strip_of(i, r):
         slot = lax.rem(i, 2)
+        at = pl.ds(pl.multiple_of(r * 32, 32), 32)
+        widened = token_v[slot, at, :].astype(F32)
+        inverse_rms = lax.rsqrt(jnp.mean(widened * widened, axis=-1, keepdims=True) + 1e-06)
+        normed[i, at, :] = (widened * inverse_rms * gain_v[...]).astype(BF16)
+
+    def norm(i, low, high):
+        def strip(r, carry):
+            strip_of(i, r)
+            return carry
+
+        lax.fori_loop(low // 32, high // 32, strip, 0, unroll=4)
+
+    def norm_tile(i):
         token_load(i).wait()
-
-        def strip(r, carry):
-            at = pl.ds(pl.multiple_of(r * 32, 32), 32)
-            widened = token_v[slot, at, :].astype(F32)
-            inverse_rms = lax.rsqrt(jnp.mean(widened * widened, axis=-1, keepdims=True) + 1e-06)
-            normed[i, at, :] = (widened * inverse_rms * gain_v[...]).astype(BF16)
-            return carry
-
-        lax.fori_loop(0, tile // 32, strip, 0, unroll=4)
+        norm(i, 0, tile)
 
     def send_chunk(send_ref, recv_ref, send_sem, recv_sem, i, chunk):
         def one(k, carry):
@@ -271,29 +283,56 @@
         others = ref.at[i, pl.ds(0, devices - 1)]
         pltpu.make_async_copy(others, others, sem.at[i]).wait()
 
-    def compute(m):
-        i, step = m // chunks, lax.rem(m, chunks)
-
-        @pl.when(step == 0)
-        def _():
-            norm(i)
-
-            @pl.when(i + 2 < tiles)
-            def _():
-                token_load(i + 2).start()
-
-        @pl.when(i == 0)
-        def _():
-            mix_load(step).wait()
-
-        n = chunk_at(i, step)
-        mixed_in = jnp.dot(normed[i], mix_v[:, wide(n)], preferred_element_type=F32).astype(BF16)
+    def project(i, n, low, high):
+        mixed_in = jnp.dot(normed[i, low:high, :], mix_v[:, wide(n)], preferred_element_type=F32).astype(BF16)
         for part in range(WIDE // GROUP_DIM):
             turned = lax.dot_general(
                 table_v[...], mixed_in[:, part * GROUP_DIM : (part + 1) * GROUP_DIM], NT,
                 preferred_element_type=F32,
             ).astype(BF16)
-            send_f[i, pl.ds(n * span + part * per_group, per_group)] = turned.reshape(per_group, channels, tile)
+            owners = pl.ds(n * span + part * per_group, per_group)
+            send_f[i, owners, :, low:high] = turned.reshape(per_group, channels, high - low)
+
+    def compute(m):
+        i, step = m // chunks, lax.rem(m, chunks)
+
+        @pl.when(step == 0)
+        def _():
+            norm_tile(i)
+
+            @pl.when(i + 2 < tiles)
+            def _():
+                token_load(i + 2).start()
+
+        @pl.when(i == 0)
+        def _():
+            mix_load(step).wait()
+
+        project(i, chunk_at(i, step), 0, tile)
+
+    def compute_half(part):
+        token_half(part).wait()
+        norm(0, part * fore, (part + 1) * fore)
+        if part == 0:
+            mix_load(0).wait()
+        project(0, chunk_first(0), part * fore, (part + 1) * fore)
+
+    def post_half(part):
+        lanes = pl.ds(part * fore, fore)
+
+        def one(k, carry):
+            there, address = partner(chunk_first(0), k)
+
+            @pl.when(there != me)
+            def _():
+                pltpu.make_async_remote_copy(
+                    src_ref=send_f.at[0, there, :, lanes], dst_ref=recv_f.at[0, me, :, lanes],
+                    send_sem=send_f_sem.at[0], recv_sem=recv_f_sem.at[0], device_id=address, device_id_type=MESH,
+                ).start()
+
+            return carry
+
+        lax.fori_loop(0, span, one, 0)
 
     def post(m):
         i, n = m // chunks, chunk_at(m // chunks, lax.rem(m, chunks))
@@ -311,6 +350,10 @@
     def forward(m, carry):
         compute(m + 1)
 
+        @pl.when(m == 0)
+        def _():
+            post_half(1)
+
         @pl.when(m > 0)
         def _():
             post(m)
@@ -320,7 +363,7 @@
     pieces = tiles * chunks
     loads[0].wait()
     loads[1].wait()
-    compute(0)
+    compute_half(0)
     for load in loads[2:]:
         load.start()
 
@@ -339,7 +382,9 @@
     def _():
         pl.semaphore_wait(barrier, 1)
 
-    post(0)
+    post_half(0)
+    compute_half(1)
+    token_load(2).start()
     lax.fori_loop(0, pieces - 1, forward, 0)
     for load in loads[2:]:
         load.wait()
@@ -508,7 +553,7 @@
         pltpu.VMEM((second * BLOCK, first), F32),
         pltpu.SemaphoreType.DMA((3 + len(constants),)),
         pltpu.SemaphoreType.DMA((mixed // WIDE,)),
-        pltpu.SemaphoreType.DMA((2,)),
+        pltpu.SemaphoreType.DMA((3,)),
         *[pltpu.SemaphoreType.DMA((tiles,)) for _ in range(4)],
         pltpu.SemaphoreType.REGULAR,
     ]

time: 191 us -> 190 us (level)
  no operation moved by 1% of the time
where the time goes in v6:
time: 190 us
  Pallas kernels  190 us (100%)
    pallas_call x1, Pallas kernels, fused(): pl.pallas_call(functools.partial(mixer_kernel, rows, cols), in_specs=[hbm...  186 us

profile of v6, /device:TPU:0, one launch (start us, length us, event | category | flops | bytes accessed | tf_op | source)
XLA Modules:
  0.0 190.0 jit_solution(9307565978538406998)
XLA Ops:
  0.0 186.4 %mixer.1 = (bf16[2,1024,2048]{2,1,0:T(8,128)(2,1)S(1)}, bf16[256,1024]{1,0:T(8,128)(2,1)S(1)}, bf16[1024,2048]{1,0:T(8,128)(2,1)S(1)}) custom-call(bf16[2,1024,2048]{2,1,0:T(8,128)(2,1)} %tokens.1, f32[1,2048]{1,0:T(1,128)} %bitcast.1, bf16[2048,1024]{1,0:T(8,128)(2,1)} %mix_in.1, bf16[2048,2048]{1,0:T(8,128)(2,1)} %gate_in.1, bf16[1024,2048]{1,0:T(8,128)(2,1)} %out_in.1, ...), custom_call_target="tpu_custom_call" | custom-call | tf_op jit(solution)/shard_map/mixer/pallas_call | solution.py:561
  186.4 3.6 %last.1 = bf16[2,1024,2048]{2,1,0:T(8,128)(2,1)} custom-call(bf16[2,1024,2048]{2,1,0:T(8,128)(2,1)S(1)} %get-tuple-element.8.gated, bf16[256,1024]{1,0:T(8,128)(2,1)S(1)} %get-tuple-element.9.left, bf16[1024,2048]{1,0:T(8,128)(2,1)S(1)} %get-tuple-element.10.out_v), custom_call_target="tpu_custom_call" | custom-call | tf_op jit(solution)/shard_map/last/pallas_call | solution.py:574
